TPU v7x, 128 devices: a whole 4x4x4 slice. The times are simulated.
128 devices in a mesh: ep: 128 (over z, y, x, core).
Axes of the slice: x: 4, y: 4, z: 4, core: 2. Of those that a mesh axis runs over, the one named last changes fastest.
Arguments:
- tokens: bfloat16 [2048, 2048], P('ep'), may hold values from -6 to 6
- recurrent_state: float32 [2048, 16, 4096], P('ep'), may hold values from -8 to 8
- first_gain: float32 [2048], replicated, may hold values from 0.1 to 1.9
- w_receptance: bfloat16 [2048, 1024], P('ep'), may hold values from -0.125 to 0.125
- w_key: bfloat16 [2048, 1024], P('ep'), may hold values from -0.125 to 0.125
- w_value: bfloat16 [2048, 1024], P('ep'), may hold values from -0.125 to 0.125
- decay_down: bfloat16 [2048, 64], replicated, may hold values from -0.125 to 0.125
- decay_up: bfloat16 [64, 1024], replicated, may hold values from -0.75 to 0.75
- decay_base: float32 [1024], replicated, may hold values from -4 to 1
- rate_down: bfloat16 [2048, 64], replicated, may hold values from -0.125 to 0.125
- rate_up: bfloat16 [64, 1024], replicated, may hold values from -0.75 to 0.75
- rate_base: float32 [1024], replicated, may hold values from -5 to 5
- key_scale: float32 [1024], replicated, may hold values from 0.25 to 4
- head_gain: float32 [1024], replicated, may hold values from 0.1 to 1.9
- w_output: bfloat16 [1024, 2048], replicated, may hold values from -0.1875 to 0.1875
- second_gain: float32 [2048], replicated, may hold values from 0.1 to 1.9
- shared_gate: bfloat16 [2048, 512], replicated, may hold values from -0.125 to 0.125
- shared_up: bfloat16 [2048, 512], replicated, may hold values from -0.125 to 0.125
- shared_down: bfloat16 [512, 2048], replicated, may hold values from -0.25 to 0.25
- expert_gate: bfloat16 [128, 2048, 512], P('ep'), may hold values from -0.125 to 0.125
- expert_up: bfloat16 [128, 2048, 512], P('ep'), may hold values from -0.125 to 0.125
- expert_down: bfloat16 [128, 512, 2048], P('ep'), may hold values from -0.25 to 0.25
- routes: int32 [2048, 4], replicated, may hold values from 0 to 127, all different within a row; in each aligned block of 16 rows (0 to 15, 16 to 31, ...) at most 4 rows name the same one
- route_weights: float32 [2048, 4], replicated, may hold values from 0.1 to 1
Outputs:
- new_tokens: bfloat16 [2048, 2048], P('ep')
- new_state: float32 [2048, 16, 4096], P('ep')
Inputs may be any that keep to these rules, and one draw needn't show every extreme that they name: `routes`: each row names 4 different experts. In the rows of one device no expert is named by more than 4 rows, a bound that some block reaches of them.
All inputs are finite; a program needn't handle non-finite values.
Results may differ from a plain program's by a relative error of at most 0.015.
Values may be sent and summed in bfloat16 or wider, within the bound.
No kernel may reach another device: no remote copies, remote signals or barrier semaphores. Data moves between devices by JAX's collectives and lax.ppermute only.
A program may use at most 128 MiB of HBM per device.

v0:
```python
import jax
import jax.numpy as jnp
from jax import lax
from jax.sharding import PartitionSpec as P

HEAD = 64
TOPK = 4
MOST = 4


NORM_EPS = 1e-06
GROUP_EPS = 0.00064


def sent_together(arrays, axis, dim, along):
    ends, at = ([], 0)
    for a in arrays[:-1]:
        at += a.shape[along]
        ends.append(at)
    both = jnp.concatenate(arrays, axis=along)
    return tuple(jnp.split(lax.all_gather(both, axis, axis=dim, tiled=True), ends, axis=along))


def rms_scale(inputs, gain):
    widened = inputs.astype(jnp.float32)
    return (
        widened * lax.rsqrt(jnp.mean(widened * widened, axis=-1, keepdims=True) + NORM_EPS) * gain
    )


def gated_units(inputs, gate_weight, up_weight):
    gate_part = jnp.dot(inputs, gate_weight, preferred_element_type=jnp.float32)
    up_part = jnp.dot(inputs, up_weight, preferred_element_type=jnp.float32)
    return (jax.nn.silu(gate_part) * up_part).astype(jnp.bfloat16)


def mix_heads(
    normed,
    receptance,
    key_rows,
    value_rows,
    state_old,
    decay_down,
    decay_up,
    decay_base,
    rate_down,
    rate_up,
    rate_base,
    key_scale,
    head_gain,
):
    count_rows = normed.shape[0]
    heads_count = state_old.shape[1]
    decay_low = jnp.tanh(jnp.dot(normed, decay_down, preferred_element_type=jnp.float32)).astype(
        jnp.bfloat16
    )
    decay_pre = decay_base + jnp.dot(decay_low, decay_up, preferred_element_type=jnp.float32)
    decay_rate = jnp.exp(-jnp.exp(-jax.nn.softplus(-decay_pre) - 0.5))
    rate_low = jnp.dot(normed, rate_down, preferred_element_type=jnp.float32).astype(jnp.bfloat16)
    learn_rate = jax.nn.sigmoid(
        rate_base + jnp.dot(rate_low, rate_up, preferred_element_type=jnp.float32)
    )

    def by_head(inputs):
        return inputs.astype(jnp.float32).reshape(count_rows, heads_count, HEAD)

    reader = by_head(receptance)
    key_heads = by_head(key_rows)
    value_heads = by_head(value_rows)
    decay_heads = by_head(decay_rate)
    learn_heads = by_head(learn_rate)
    scaled = key_heads * key_scale.reshape(heads_count, HEAD)
    direction = scaled / jnp.sqrt(jnp.sum(scaled * scaled, axis=-1, keepdims=True) + 1.0)
    state_prev = state_old.reshape(count_rows, heads_count, HEAD, HEAD)
    removed = jnp.sum(state_prev * direction[:, :, None, :], axis=-1)
    state_next = (
        state_prev * decay_heads[:, :, None, :]
        - removed[..., None] * (direction * learn_heads)[:, :, None, :]
        + value_heads[..., None] * key_heads[:, :, None, :]
    )
    readout = jnp.sum(state_next * reader[:, :, None, :], axis=-1)
    centre = jnp.mean(readout, axis=-1, keepdims=True)
    spread = jnp.mean(jnp.square(readout - centre), axis=-1, keepdims=True)
    normalized = ((readout - centre) * lax.rsqrt(spread + GROUP_EPS)).reshape(
        count_rows, heads_count * HEAD
    )
    normalized = normalized * head_gain
    return (
        normalized.astype(jnp.bfloat16),
        state_next.reshape(count_rows, heads_count, HEAD * HEAD),
    )


def per_device(
    tokens,
    recurrent_state,
    first_gain,
    w_receptance,
    w_key,
    w_value,
    decay_down,
    decay_up,
    decay_base,
    rate_down,
    rate_up,
    rate_base,
    key_scale,
    head_gain,
    w_output,
    second_gain,
    shared_gate,
    shared_up,
    shared_down,
    expert_gate,
    expert_up,
    expert_down,
    routes,
    route_weights,
):
    local_rows = tokens.shape[0]
    width = tokens.shape[1]
    normed = rms_scale(tokens, first_gain).astype(jnp.bfloat16)
    weight_rows = sent_together((w_receptance, w_key, w_value), "ep", 0, 1)
    columns = normed
    recept_sum = jnp.dot(columns, weight_rows[0], preferred_element_type=jnp.float32)
    key_sum = jnp.dot(columns, weight_rows[1], preferred_element_type=jnp.float32)
    value_sum = jnp.dot(columns, weight_rows[2], preferred_element_type=jnp.float32)
    mixed, new_state = mix_heads(
        normed,
        recept_sum.astype(jnp.bfloat16),
        key_sum.astype(jnp.bfloat16),
        value_sum.astype(jnp.bfloat16),
        recurrent_state,
        decay_down,
        decay_up,
        decay_base,
        rate_down,
        rate_up,
        rate_base,
        key_scale,
        head_gain,
    )
    residual = (
        tokens.astype(jnp.float32) + jnp.dot(mixed, w_output, preferred_element_type=jnp.float32)
    ).astype(jnp.bfloat16)
    second = rms_scale(residual, second_gain).astype(jnp.bfloat16)
    shared = jnp.dot(
        gated_units(second, shared_gate, shared_up), shared_down, preferred_element_type=jnp.float32
    )
    my_expert = lax.axis_index("ep")
    devices = lax.axis_size("ep")
    own_start = my_expert * local_rows
    own_routes = lax.dynamic_slice_in_dim(routes, own_start, local_rows, 0)
    own_weights = lax.dynamic_slice_in_dim(route_weights, own_start, local_rows, 0)
    flat_expert = own_routes.reshape(-1)
    assigned = flat_expert.shape[0]
    order_index = jnp.arange(assigned, dtype=jnp.int32)
    earlier = (flat_expert[:, None] == flat_expert[None, :]) & (
        order_index[None, :] < order_index[:, None]
    )
    slot_index = jnp.sum(earlier.astype(jnp.int32), axis=1)
    place = flat_expert * MOST + slot_index
    source_rows = jnp.repeat(second, TOPK, axis=0)
    outgoing = jnp.zeros((devices * MOST, width), jnp.bfloat16).at[place].set(source_rows)
    outgoing = outgoing.reshape(devices, MOST, width)
    received = lax.all_to_all(outgoing, "ep", split_axis=0, concat_axis=0, tiled=True)
    senders, slots_here, columns = received.shape
    hidden = gated_units(
        received.reshape(senders * slots_here, columns), expert_gate[0], expert_up[0]
    )
    produced = (
        jnp.dot(hidden, expert_down[0], preferred_element_type=jnp.float32)
        .astype(jnp.bfloat16)
        .reshape(senders, slots_here, columns)
    )
    returned = lax.all_to_all(produced, "ep", split_axis=0, concat_axis=0, tiled=True)
    answers = returned.reshape(devices * MOST, width)[place].reshape(local_rows, TOPK, width)
    routed = jnp.sum(answers.astype(jnp.float32) * own_weights[:, :, None], axis=1)
    new_tokens = (residual.astype(jnp.float32) + shared + routed).astype(jnp.bfloat16)
    return (new_tokens, new_state)


def solution(mesh):
    in_specs = (
        P("ep", None),
        P("ep", None, None),
        P(),
        P("ep", None),
        P("ep", None),
        P("ep", None),
        P(),
        P(),
        P(),
        P(),
        P(),
        P(),
        P(),
        P(),
        P(),
        P(),
        P(),
        P(),
        P(),
        P("ep", None, None),
        P("ep", None, None),
        P("ep", None, None),
        P(),
        P(),
    )
    out_specs = (P("ep", None), P("ep", None, None))
    return jax.shard_map(
        per_device, mesh=mesh, in_specs=in_specs, out_specs=out_specs, check_vma=False
    )
```

profile of v0, /device:TPU:1, one launch (start us, length us, event | category | flops | bytes accessed | tf_op | source)
XLA Modules:
  0.0 295.3 jit_solution(12814744326719932283)
XLA Ops:
  7.2 0.0 copy-start
  7.2 0.0 all-gather.2.cloned.1.call-start
  7.2 1.6 pad_maximum_fusion
  8.8 0.0 all-gather.2.cloned.1.call-update
  8.8 0.8 mul.217
  9.6 1.0 fusion.56
  10.6 1.5 fusion.29
  12.1 0.1 reshape.148
  12.1 1.5 fusion.63
  13.7 0.1 mul.214
  13.8 7.8 %reshape.145 = f32[16,16,64,64]{3,2,1,0:T(8,128)} reshape(f32[16,16,4096]{2,1,0:T(8,128)} %param.25) | data formatting | bytes 8388608 | tf_op jit(solution)/shard_map/reshape | solution.py:74
  21.6 3.8 %mul.215 = f32[16,16,64,64]{3,2,1,0:T(8,128)} broadcast(f32[16,16,64]{2,1,0:T(8,128)S(1)} %mul.214), dimensions={0,1,3} | broadcast | bytes 4259840 | tf_op jit(solution)/shard_map/mul | solution.py:77
  25.4 0.0 copy-start.1
  25.4 8.0 %mul.236 = f32[16,16,4096]{2,1,0:T(8,128)} reshape(f32[16,16,64,64]{3,2,1,0:T(8,128)} %mul.215) | data formatting | bytes 8388608 | tf_op jit(solution)/shard_map/mul | solution.py:77
  33.4 0.8 broadcast_multiply_fusion.3
  34.1 0.1 copy.33
  34.2 0.1 eq.15
  34.3 0.1 copy.32
  34.4 0.1 mul.257
  34.5 0.2 convert_reduce_fusion
  34.7 53.7 %all-gather.2.cloned.1.call-done = bf16[2048,3072]{1,0:T(8,128)(2,1)} async-done(((bf16[16,3072]{1,0:T(8,128)(2,1)}), bf16[2048,3072]{1,0:T(8,128)(2,1)}) %all-gather.2.cloned.1.call-update) | async-done | bytes 12582928 | tf_op jit(solution)/shard_map/all_gather | solution.py:21
  88.4 0.0 copy-done.1
  88.4 0.0 copy-done.2
  88.4 2.9 fusion.34
  91.3 0.1 reshape.155
  91.4 0.1 multiply_reduce_fusion.6
  91.5 2.9 fusion.46
  94.4 0.1 reshape.157
  94.5 2.9 fusion.40
  97.4 0.1 reshape.156
  97.5 0.1 fusion.82
  97.6 39.6 %broadcast_multiply_fusion = (f32[16,16,64,64]{3,2,1,0:T(8,128)}, f32[16,16,64]{2,1,0:T(8,128)S(1)}, f32[16,16,64,64]{3,2,1,0:T(8,128)}) fusion(f32[16,16,64]{2,1,0:T(8,128)S(1)} %reshape.155, f32[16,16,64]{2,1,0:T(8,128)S(1)} %reshape.156, f32[16,16,64]{2,1,0:T(8,128)S(1)} %reshape.157, f32[16,16,64,64]{3,2,1,0:T(8,128)} %reshape.145, ...), kind=kOutput, calls=%fused_computation.14 | output fusion | flops 8388671 | bytes 13041664 | tf_op jit(solution)/shard_map/mul | solution.py:78
  137.2 7.9 %mul.238 = f32[16,16,4096]{2,1,0:T(8,128)} reshape(f32[16,16,64,64]{3,2,1,0:T(8,128)} %get-tuple-element.10) | data formatting | bytes 8388608 | tf_op jit(solution)/shard_map/mul | solution.py:78
  145.1 7.9 %mul.239 = f32[16,16,4096]{2,1,0:T(8,128)} reshape(f32[16,16,64,64]{3,2,1,0:T(8,128)} %get-tuple-element.8) | data formatting | bytes 8388608 | tf_op jit(solution)/shard_map/mul | solution.py:79
  153.0 3.8 %mul.234 = f32[16,16,64,64]{3,2,1,0:T(8,128)} broadcast(f32[16,16,64]{2,1,0:T(8,128)S(1)} %reshape.157), dimensions={0,1,3} | broadcast | bytes 4259840 | tf_op jit(solution)/shard_map/mul | solution.py:81
  156.8 7.9 %mul.240 = f32[16,16,4096]{2,1,0:T(8,128)} reshape(f32[16,16,64,64]{3,2,1,0:T(8,128)} %mul.234) | data formatting | bytes 8388608 | tf_op jit(solution)/shard_map/mul | solution.py:81
  164.7 10.0 %multiply_reduce_fusion.2 = (f32[16,16]{1,0:T(8,128)S(1)}, f32[16,16,4096]{2,1,0:T(8,128)}) fusion(f32[16,16,4096]{2,1,0:T(8,128)} %mul.240, f32[16,16,4096]{2,1,0:T(8,128)} %mul.239, f32[16,16,4096]{2,1,0:T(8,128)} %mul.238, f32[16,16,4096]{2,1,0:T(8,128)} %param.25, f32[16,16,4096]{2,1,0:T(8,128)} %mul.236), kind=kLoop, calls=%fused_computation.12 | loop fusion | flops 5242624 | bytes 25166848 | tf_op jit(solution)/shard_map/reduce_sum | solution.py:82
  174.6 0.2 multiply_reduce_fusion.5
  174.8 0.1 subtract_multiply_fusion
  175.0 0.1 mul.244
  175.1 0.0 copy-done.4
  175.1 3.0 %multiply_reduce_fusion.4 = (f32[16]{0:T(128)S(1)}, f32[16,2048]{1,0:T(8,128)S(1)}) fusion(bf16[1024,2048]{1,0:T(8,128)(2,1)} %param.38, f32[16,1024]{1,0:T(8,128)S(1)} %mul.244, f32[1024]{0:T(1024)S(1)} %copy-done.4, bf16[16,2048]{1,0:T(8,128)(2,1)S(1)} %copy-done.1), kind=kOutput, calls=%fused_computation.60 | convolution fusion | flops 67338224 | bytes 4460608 | tf_op jit(solution)/shard_map/dot_general | solution.py:144
  178.1 0.0 copy-done.3
  178.1 0.1 multiply_convert_fusion
  178.2 0.1 broadcast_in_dim.5
  178.3 0.1 reshape.171
  178.3 2.7 scatter_custom_fusion
  181.0 4.1 %reshape.150 = bf16[128,4,2048]{2,1,0:T(4,128)(2,1)} reshape(bf16[512,2048]{1,0:T(8,128)(2,1)} %scatter_custom_fusion) | data formatting | bytes 4194304 | tf_op jit(solution)/shard_map/reshape | solution.py:165
  185.1 37.9 %all_to_all.10 = bf16[128,4,2048]{2,1,0:T(4,128)(2,1)} all-to-all(bf16[128,4,2048]{2,1,0:T(4,128)(2,1)} %reshape.150), channel_id=1, replica_groups=mesh['ep'=128] {'ep'}, dimensions={0} | all-to-all | bytes 4194304 | tf_op jit(solution)/shard_map/all_to_all | solution.py:166
  223.0 4.0 %reshape.151 = bf16[512,2048]{1,0:T(8,128)(2,1)} reshape(bf16[128,4,2048]{2,1,0:T(4,128)(2,1)} %all_to_all.10) | data formatting | bytes 4194304 | tf_op jit(solution)/shard_map/reshape | solution.py:169
  227.0 4.4 %fusion.18 = f32[512,512]{1,0:T(8,128)} fusion(bf16[512,2048]{1,0:T(8,128)(2,1)} %reshape.151, bf16[1,2048,512]{2,1,0:T(8,128)(2,1)} %param.43), kind=kOutput, calls=%fused_computation.27 | convolution fusion | flops 1073741824 | bytes 5242880 | tf_op jit(solution)/shard_map/dot_general | solution.py:32
  231.4 0.0 copy-done
  231.4 6.2 %convolution_convert_fusion = bf16[512,2048]{1,0:T(8,128)(2,1)} fusion(bf16[1,512,2048]{2,1,0:T(8,128)(2,1)S(1)} %copy-done, bf16[512,2048]{1,0:T(8,128)(2,1)} %reshape.151, bf16[1,2048,512]{2,1,0:T(8,128)(2,1)} %param.44, f32[512,512]{1,0:T(8,128)} %fusion.18), kind=kOutput, calls=%fused_computation.17 | convolution fusion | flops 2150105088 | bytes 9437184 | tf_op jit(solution)/shard_map/dot_general | solution.py:172
  237.6 4.1 %reshape.152 = bf16[128,4,2048]{2,1,0:T(4,128)(2,1)} reshape(bf16[512,2048]{1,0:T(8,128)(2,1)} %convolution_convert_fusion) | data formatting | bytes 4194304 | tf_op jit(solution)/shard_map/reshape | solution.py:174
  241.8 5.5 %all-to-all-start.1 = ((bf16[128,4,2048]{2,1,0:T(4,128)(2,1)}), bf16[128,4,2048]{2,1,0:T(4,128)(2,1)}, u32[]{:S(2)}, u32[]{:S(2)}) async-start(bf16[128,4,2048]{2,1,0:T(4,128)(2,1)} %reshape.152), calls=%async_computation.1 | async-start | bytes 4194304 | tf_op jit(solution)/shard_map/all_to_all | solution.py:176
  247.2 0.8 constant_dynamic-slice_fusion
  248.0 0.1 copy.34
  248.1 2.0 fusion.83
  250.0 27.4 %all-to-all-done.1 = bf16[128,4,2048]{2,1,0:T(4,128)(2,1)} async-done(((bf16[128,4,2048]{2,1,0:T(4,128)(2,1)}), bf16[128,4,2048]{2,1,0:T(4,128)(2,1)}, u32[]{:S(2)}, u32[]{:S(2)}) %all-to-all-start.1) | async-done | bytes 2097184 | tf_op jit(solution)/shard_map/all_to_all | solution.py:176
  277.5 4.0 %reshape.153 = bf16[512,2048]{1,0:T(8,128)(2,1)} reshape(bf16[128,4,2048]{2,1,0:T(4,128)(2,1)} %all-to-all-done.1) | data formatting | bytes 4194304 | tf_op jit(solution)/shard_map/reshape | solution.py:177
  281.4 2.8 gather_fusion
  284.3 0.2 reshape.158
  284.5 0.4 multiply_reduce_fusion.3
  284.9 3.6 %fusion.14 = bf16[16,2048]{1,0:T(8,128)(2,1)} fusion(f32[16,2048]{1,0:T(8,128)S(1)} %multiply_reduce_fusion.3, f32[16,2048]{1,0:T(8,128)S(1)} %get-tuple-element.12, bf16[512,2048]{1,0:T(8,128)(2,1)} %param.42, bf16[16,2048]{1,0:T(8,128)(2,1)S(1)} %multiply_convert_fusion, bf16[2048,512]{1,0:T(8,128)(2,1)} %param.41, f32[16,512]{1,0:T(8,128)S(1)} %fusion.83), kind=kOutput, calls=%fused_computation.23 | convolution fusion | flops 67256320 | bytes 4620288 | tf_op jit(solution)/shard_map/dot_general | solution.py:147
  (10 shorter events, 0.0 us)
Async XLA Ops:
  7.2 224.3 %copy-start = (bf16[1,512,2048]{2,1,0:T(8,128)(2,1)S(1)}, bf16[1,512,2048]{2,1,0:T(8,128)(2,1)}, u32[]{:S(2)}) copy-start(bf16[1,512,2048]{2,1,0:T(8,128)(2,1)} %param.45) | copy-start | bytes 6291460
  7.2 81.2 %all-gather.2.cloned.1.call-start = ((), (), s32[]{:S(2)}) async-start(), calls=%async_computation.2 | async-start | bytes 12681216 | tf_op jit(solution)/shard_map/all_gather | solution.py:21
  25.4 63.0 %copy-start.1 = (bf16[16,2048]{1,0:T(8,128)(2,1)S(1)}, bf16[16,2048]{1,0:T(8,128)(2,1)}, u32[]{:S(2)}) copy-start(bf16[16,2048]{1,0:T(8,128)(2,1)} %param.24) | copy-start | bytes 196612
  25.4 63.0 %copy-start.2 = (f32[2048]{0:T(1024)S(1)}, f32[2048]{0:T(1024)}, u32[]{:S(2)}) copy-start(f32[2048]{0:T(1024)} %param.26) | copy-start | bytes 24580
  164.7 10.4 %copy-start.4 = (f32[1024]{0:T(1024)S(1)}, f32[1024]{0:T(1024)}, u32[]{:S(2)}) copy-start(f32[1024]{0:T(1024)} %param.37) | copy-start | bytes 12292
  174.6 3.4 %copy-start.3 = (f32[2048]{0:T(1024)S(1)}, f32[2048]{0:T(1024)}, u32[]{:S(2)}) copy-start(f32[2048]{0:T(1024)} %param.39) | copy-start | bytes 24580
  241.8 35.7 %all-to-all-start.1 = ((bf16[128,4,2048]{2,1,0:T(4,128)(2,1)}), bf16[128,4,2048]{2,1,0:T(4,128)(2,1)}, u32[]{:S(2)}, u32[]{:S(2)}) async-start(bf16[128,4,2048]{2,1,0:T(4,128)(2,1)} %reshape.152), calls=%async_computation.1 | async-start | bytes 4194304 | tf_op jit(solution)/shard_map/all_to_all | solution.py:176
Sparse Core Ops, SparseCore 0:
  11.7 76.6 all-gather.1
where the time goes:
time: 297 us; the launch traced here: 295 us
  waiting for transfers between devices  81.2 us (27%)
  local copies, waits for them, and re-layouts  71.6 us (24%)
  other arithmetic  54.1 us (18%)
  blocking collectives  37.9 us (13%)
  matrix products  30.8 us (10%)
  between operations  14.2 us (5%)
  starting transfers between devices  5.5 us (2%)
    all_gather x1, waiting for transfers between devices, sent_together(): lax.all_gather(both, axis, axis=dim, tiled=True)  53.7 us
    mul x1, other arithmetic, mix_heads(): removed[..., None] * (direction * learn_heads)[:, :, None, :]  39.6 us
    all_to_all x1, blocking collectives, per_device(): lax.all_to_all(outgoing, 'ep', split_axis=0, concat_axis=0, tiled=True)  37.9 us
    all_to_all x1, waiting for transfers between devices, per_device(): lax.all_to_all(produced, 'ep', split_axis=0, concat_axis=0, tiled=True)  27.4 us
    mul x3, local copies, waits for them, and re-layouts, mix_heads(): state_prev * decay_heads[:, :, None, :]  11.9 us
    mul x3, local copies, waits for them, and re-layouts, mix_heads(): readout = jnp.sum(state_next * reader[:, :, None, :], axis=-1)  11.7 us
    reduce_sum x1, other arithmetic, mix_heads(): centre = jnp.mean(readout, axis=-1, keepdims=True)  9.97 us
    mul x2, local copies, waits for them, and re-layouts, mix_heads(): value_heads[..., None] * key_heads[:, :, None, :]  8.01 us
  transfers between devices with their start and end apart: 2, of which 2 were waited for; matrix products, arithmetic and copies ran while one was open for 10% of the time, Pallas kernels for 0%

commit v1 on v0

v1 whole, which is shorter than its diff:
```python
import jax
import jax.numpy as jnp
from jax import lax
from jax.experimental import pallas as pl
from jax.experimental.pallas import tpu as pltpu
from jax.sharding import PartitionSpec as P

HEAD = 64
MOST = 4
HALVES = 2
NORM_EPS = 1e-06
GROUP_EPS = 0.00064
BF = jnp.bfloat16
F32 = jnp.float32


def sent_together(arrays, axis, dim, along):
    ends, at = ([], 0)
    for a in arrays[:-1]:
        at += a.shape[along]
        ends.append(at)
    both = jnp.concatenate(arrays, axis=along)
    return tuple(jnp.split(lax.all_gather(both, axis, axis=dim, tiled=True), ends, axis=along))


def rms_scale(inputs, gain):
    widened = inputs.astype(F32)
    return (
        widened * lax.rsqrt(jnp.mean(widened * widened, axis=-1, keepdims=True) + NORM_EPS) * gain
    )


def dot32(a, b):
    return jnp.dot(a, b, preferred_element_type=F32)


def gated_units(inputs, gate_weight, up_weight):
    return (jax.nn.silu(dot32(inputs, gate_weight)) * dot32(inputs, up_weight)).astype(BF)


def high_low(x):
    high = x.astype(BF)
    return high, (x - high.astype(F32)).astype(BF)


def mix_kernel(vec_ref, gain_ref, state_ref, spread_ref, fold_ref, mixed_ref, next_ref):
    rows = state_ref.shape[0]
    heads = state_ref.shape[1]
    lanes = state_ref.shape[2]
    chunk = 1024
    both = rows * heads

    def part(i):
        return vec_ref[:, i].reshape(both, HEAD)

    def twice(x):
        return jnp.concatenate([x, x], axis=1)

    reader, key, value, decay, learn, scale = (part(i) for i in range(6))
    scaled = key * scale
    direction = scaled / jnp.sqrt(jnp.sum(scaled * scaled, axis=-1, keepdims=True) + 1.0)
    decay2 = twice(decay)
    key2 = twice(key)
    reader2 = twice(reader)
    dir2 = twice(direction)
    taken2 = twice(direction * learn)
    removed = jnp.zeros((both, HEAD), F32)
    for c in range(lanes // chunk):
        pieces = []
        for j in range(chunk // 128):
            at = c * chunk + j * 128
            pieces.append(state_ref[:, :, at : at + 128].reshape(both, 128) * dir2)
        product = jnp.concatenate(pieces, axis=1)
        high, low = high_low(product)
        fold = fold_ref[c * chunk : (c + 1) * chunk, :]
        removed = removed + dot32(high, fold) + dot32(low, fold)
    high, low = high_low(removed)
    known = jnp.concatenate([high, low], axis=1)
    value = value.astype(BF)
    readout = jnp.zeros((both, HEAD), F32)
    for c in range(lanes // chunk):
        spread = spread_ref[:, c * chunk : (c + 1) * chunk]
        removed_wide = dot32(known, jnp.concatenate([spread, spread], axis=0))
        value_wide = dot32(value, spread)
        pieces = []
        for j in range(chunk // 128):
            at = c * chunk + j * 128
            sub = slice(j * 128, j * 128 + 128)
            state = (
                state_ref[:, :, at : at + 128].reshape(both, 128) * decay2
                - removed_wide[:, sub] * taken2
                + value_wide[:, sub] * key2
            )
            next_ref[:, :, at : at + 128] = state.reshape(rows, heads, 128)
            pieces.append(state * reader2)
        product = jnp.concatenate(pieces, axis=1)
        high, low = high_low(product)
        fold = fold_ref[c * chunk : (c + 1) * chunk, :]
        readout = readout + dot32(high, fold) + dot32(low, fold)
    centre = jnp.mean(readout, axis=-1, keepdims=True)
    apart = readout - centre
    spread_var = jnp.mean(apart * apart, axis=-1, keepdims=True)
    gain = jnp.broadcast_to(gain_ref[...][None], (rows, heads, HEAD)).reshape(both, HEAD)
    mixed = apart * lax.rsqrt(spread_var + GROUP_EPS) * gain
    mixed_ref[...] = mixed.reshape(rows, heads, HEAD)


def mix_heads(vectors, head_gain, state_old):
    count, heads, lanes = state_old.shape
    rows = 4
    lane = jnp.arange(lanes, dtype=jnp.int32)
    entry = jnp.arange(HEAD, dtype=jnp.int32)
    spread = (entry[:, None] == lane[None, :] // HEAD).astype(BF)
    fold = (lane[:, None] // HEAD == entry[None, :]).astype(BF)
    return pl.pallas_call(
        mix_kernel,
        grid=(count // rows,),
        in_specs=[
            pl.BlockSpec((rows, 6, heads, HEAD), lambda i: (i, 0, 0, 0)),
            pl.BlockSpec((heads, HEAD), lambda i: (0, 0)),
            pl.BlockSpec((rows, heads, lanes), lambda i: (i, 0, 0)),
            pl.BlockSpec((HEAD, lanes), lambda i: (0, 0)),
            pl.BlockSpec((lanes, HEAD), lambda i: (0, 0)),
        ],
        out_specs=[
            pl.BlockSpec((rows, heads, HEAD), lambda i: (i, 0, 0)),
            pl.BlockSpec((rows, heads, lanes), lambda i: (i, 0, 0)),
        ],
        out_shape=[
            jax.ShapeDtypeStruct((count, heads, HEAD), F32),
            jax.ShapeDtypeStruct((count, heads, lanes), F32),
        ],
        name="mix",
    )(vectors, head_gain.reshape(heads, HEAD), state_old, spread, fold)


def per_device(
    tokens,
    recurrent_state,
    first_gain,
    w_receptance,
    w_key,
    w_value,
    decay_down,
    decay_up,
    decay_base,
    rate_down,
    rate_up,
    rate_base,
    key_scale,
    head_gain,
    w_output,
    second_gain,
    shared_gate,
    shared_up,
    shared_down,
    expert_gate,
    expert_up,
    expert_down,
    routes,
    route_weights,
):
    rows, width = tokens.shape
    heads = recurrent_state.shape[1]
    mix = w_key.shape[1]
    half = width // HALVES
    devices = lax.axis_size("ep")
    my_expert = lax.axis_index("ep")

    own_routes = lax.dynamic_slice_in_dim(routes, my_expert * rows, rows, 0)
    own_weights = lax.dynamic_slice_in_dim(route_weights, my_expert * rows, rows, 0)
    place = jnp.arange(devices * MOST * HALVES, dtype=jnp.int32)
    named = own_routes[:, :, None] == (place // (MOST * HALVES))[None, None, :]
    weight = jnp.sum(jnp.where(named, own_weights[:, :, None], 0.0), axis=1)
    named = jnp.any(named, axis=1)
    order = jnp.arange(rows, dtype=jnp.int32)
    before = (order[None, :] < order[:, None]).astype(BF)
    slot = dot32(before, named.astype(BF))
    chosen = named & (slot == (place % MOST)[None, :].astype(F32))
    side = (place // MOST) % HALVES
    picks = [chosen & (side == h)[None, :] for h in range(HALVES)]
    pick = jnp.concatenate(picks, axis=0).astype(BF)
    weigh_high, weigh_low = high_low(
        jnp.concatenate([jnp.where(p, weight, 0.0) for p in picks], axis=0)
    )
    weigh = jnp.concatenate([weigh_high, weigh_low], axis=0)

    normed = rms_scale(tokens, first_gain).astype(BF)
    decay_low = jnp.tanh(dot32(normed, decay_down)).astype(BF)
    decay_pre = decay_base + dot32(decay_low, decay_up)
    decay_rate = jnp.exp(-jnp.exp(-jax.nn.softplus(-decay_pre) - 0.5))
    rate_low = dot32(normed, rate_down).astype(BF)
    learn_rate = jax.nn.sigmoid(rate_base + dot32(rate_low, rate_up))

    weight_rows = sent_together((w_receptance, w_key, w_value), "ep", 0, 1)
    reader, key_rows, value_rows = (
        dot32(normed, w).astype(BF).astype(F32) for w in weight_rows
    )
    vectors = jnp.stack(
        [
            reader,
            key_rows,
            value_rows,
            decay_rate,
            learn_rate,
            jnp.broadcast_to(key_scale[None, :], (rows, mix)),
        ],
        axis=1,
    ).reshape(rows, 6, heads, HEAD)
    mixed, new_state = mix_heads(vectors, head_gain, recurrent_state)
    mixed = mixed.reshape(rows, mix).astype(BF)
    residual = (tokens.astype(F32) + dot32(mixed, w_output)).astype(BF)
    second = rms_scale(residual, second_gain).astype(BF)

    halves = jnp.concatenate([second[:, :half], second[:, half:]], axis=0)
    outgoing = lax.dot_general(pick, halves, (((0,), (0,)), ((), ()))).astype(BF)
    received = lax.all_to_all(
        outgoing.reshape(devices, MOST * HALVES, half), "ep", split_axis=0, concat_axis=0, tiled=True
    ).reshape(devices * MOST * HALVES, half)
    shared = dot32(gated_units(second, shared_gate, shared_up), shared_down)

    block = 256
    blocks = devices * MOST * HALVES // block
    kept = block // HALVES
    source = jnp.arange(block, dtype=jnp.int32)
    target = jnp.arange(kept, dtype=jnp.int32)
    at = target // MOST * (MOST * HALVES) + target % MOST
    unchunk = [(at[:, None] + MOST * h == source[None, :]).astype(BF) for h in range(HALVES)]
    chunks = received.reshape(blocks, block, half)
    inputs = jnp.concatenate(
        [
            jnp.einsum("pq,bqc->bpc", u, chunks, preferred_element_type=F32).astype(BF)
            for u in unchunk
        ],
        axis=2,
    ).reshape(devices * MOST, width)
    hidden = gated_units(inputs, expert_gate[0], expert_up[0])
    hidden = hidden.reshape(blocks, kept, hidden.shape[1])
    spread = [
        jnp.einsum("pq,bpc->bqc", u, hidden, preferred_element_type=F32).astype(BF)
        for u in unchunk
    ]
    down = expert_down[0]
    produced = dot32(
        jnp.concatenate(spread, axis=2).reshape(devices * MOST * HALVES, -1),
        jnp.concatenate([down[:, :half], down[:, half:]], axis=0),
    ).astype(BF)
    returned = lax.all_to_all(
        produced.reshape(devices, MOST * HALVES, half), "ep", split_axis=0, concat_axis=0, tiled=True
    ).reshape(devices * MOST * HALVES, half)
    parts = dot32(weigh, returned).reshape(2, HALVES, rows, half)
    parts = parts[0] + parts[1]
    routed = jnp.concatenate([parts[0], parts[1]], axis=1)
    new_tokens = (residual.astype(F32) + shared + routed).astype(BF)
    return (new_tokens, new_state)


def solution(mesh):
    row = P("ep", None)
    block = P("ep", None, None)
    whole = P()
    in_specs = (
        (row, block, whole, row, row, row)
        + (whole,) * 13
        + (block, block, block, whole, whole)
    )
    return jax.shard_map(
        per_device, mesh=mesh, in_specs=in_specs, out_specs=(row, block), check_vma=False
    )
```

time: 297 us -> 226 us (0.76)
  local copies, waits for them, and re-layouts: 71.6 us -> 16 us
  other arithmetic: 54.1 us -> 9.02 us
  waiting for transfers between devices: 81.2 us -> 123 us
  blocking collectives: 37.9 us -> 0 us
  Pallas kernels: 0 us -> 10.6 us
  matrix products: 30.8 us -> 39.3 us
  starting transfers between devices: 5.5 us -> 12.4 us
    mul x4 -> x0, other arithmetic: 40.6 us -> none  [the longest x1 39.6 us: mix_heads(): removed[..., None] * (direction * learn_heads)[:, :, None, :]]
    mul x13 -> x0, local copies, waits for them, and re-layouts: 40.5 us -> none  [the longest x3 11.9 us: mix_heads(): state_prev * decay_heads[:, :, None, :]]
    all_to_all x1 -> x0, blocking collectives: 37.9 us -> none  [per_device(): lax.all_to_all(outgoing, 'ep', split_axis=0, concat_axis=0, tiled=True)]
    all_to_all x1 -> x2, waiting for transfers between devices: 27.4 us -> 56 us  [the longest x1 28.6 us: per_device(): lax.all_to_all(produced.reshape(devices, MOST * HALVES, half), 'ep', spli...]
    reshape x8 -> x1, local copies, waits for them, and re-layouts: 24.2 us -> 1.35 us  [mix_heads(): head_gain.reshape(heads, HEAD)]
    all_gather x1, waiting for transfers between devices: 53.7 us -> 67.1 us  [sent_together(): lax.all_gather(both, axis, axis=dim, tiled=True)]
    reduce_sum x5 -> x1, other arithmetic: 10.8 us -> 0.09 us  [per_device(): weight = jnp.sum(jnp.where(named, own_weights[:, :, None], 0.0), axis=1)]
    pallas_call x0 -> x1, Pallas kernels: none -> 10.6 us  [mix_heads(): pl.pallas_call(mix_kernel, grid=(count // rows,), in_specs=[pl.BlockSpec(...]
  transfers between devices with their start and end apart: 2 -> 3, of which waited for: 2 -> 3; matrix products, arithmetic and copies ran while one was open for 10% -> 8% of each run, Pallas kernels for 0% -> 0%
where the time goes in v1:
time: 226 us; the launch traced here: 225 us
  waiting for transfers between devices  123 us (54%)
  matrix products  39.3 us (17%)
  local copies, waits for them, and re-layouts  16 us (7%)
  between operations  14.4 us (6%)
  starting transfers between devices  12.4 us (5%)
  Pallas kernels  10.6 us (5%)
  other arithmetic  9.02 us (4%)
    all_gather x1, waiting for transfers between devices, sent_together(): lax.all_gather(both, axis, axis=dim, tiled=True)  67.1 us
    dot_general x13, matrix products, dot32(): return jnp.dot(a, b, preferred_element_type=F32)  31.5 us
    all_to_all x1, waiting for transfers between devices, per_device(): lax.all_to_all(produced.reshape(devices, MOST * HALVES, half), 'ep', spli...  28.6 us
    all_to_all x1, waiting for transfers between devices, per_device(): lax.all_to_all(outgoing.reshape(devices, MOST * HALVES, half), 'ep', spli...  27.4 us
    pallas_call x1, Pallas kernels, mix_heads(): pl.pallas_call(mix_kernel, grid=(count // rows,), in_specs=[pl.BlockSpec(...  10.6 us
    all_to_all x1, starting transfers between devices, per_device(): lax.all_to_all(outgoing.reshape(devices, MOST * HALVES, half), 'ep', spli...  7.83 us
    dot_general x2, matrix products, per_device(): jnp.einsum('pq,bqc->bpc', u, chunks, preferred_element_type=F32).astype(BF)  4.78 us
    all_to_all x1, starting transfers between devices, per_device(): lax.all_to_all(produced.reshape(devices, MOST * HALVES, half), 'ep', spli...  4.52 us
  transfers between devices with their start and end apart: 3, of which 3 were waited for; matrix products, arithmetic and copies ran while one was open for 8% of the time, Pallas kernels for 0%

profile of v1, /device:TPU:1, one launch (start us, length us, event | category | flops | bytes accessed | tf_op | source)
XLA Modules:
  0.0 224.8 jit_solution(9935412299536794987)
XLA Ops:
  7.2 0.0 copy-start
  7.2 0.0 copy-start.3
  7.2 0.0 copy-start.6
  7.2 0.0 all-gather.2.cloned.1.call-start
  7.3 1.6 pad_maximum_fusion.3
  8.8 0.0 all-gather.2.cloned.1.call-update
  8.9 0.8 stack_broadcast_in_dim.7
  9.6 1.3 reshape.227.gain_ref
  11.0 1.0 fusion.61
  11.9 1.5 fusion.81
  13.5 0.1 stack.30
  13.6 1.5 fusion.36
  15.0 0.1 stack.31
  15.1 0.8 constant_dynamic-slice_fusion.1
  15.9 0.8 constant_dynamic-slice_fusion
  16.7 0.1 compare_reduce_fusion
  16.8 0.1 fusion.60
  16.9 0.8 broadcast_select_fusion.1
  17.7 0.9 fusion.59.spread_ref
  18.6 2.7 %fusion.20.fold_ref = bf16[4096,64]{1,0:T(8,128)(2,1)} fusion(s32[4096]{0:T(1024)S(1)} %add_select_fusion), kind=kLoop, calls=%fused_computation.26 | loop fusion | flops 524288 | bytes 540672 | tf_op jit(solution)/shard_map/convert_element_type | solution.py:114
  21.3 67.1 %all-gather.2.cloned.1.call-done = bf16[2048,3072]{1,0:T(8,128)(2,1)} async-done(((bf16[16,3072]{1,0:T(8,128)(2,1)}), bf16[2048,3072]{1,0:T(8,128)(2,1)}) %all-gather.2.cloned.1.call-update) | async-done | bytes 12582928 | tf_op jit(solution)/shard_map/all_gather | solution.py:23
  88.4 0.0 copy-done.3
  88.4 0.0 copy-done.6
  88.4 2.9 %fusion.53 = f32[16,1024]{1,0:T(8,128)S(1)} fusion(bf16[2048,3072]{1,0:T(8,128)(2,1)} %all-gather.2.cloned.1.call-done, bf16[16,2048]{1,0:T(8,128)(2,1)S(1)} %copy-done.3, f32[2048]{0:T(1024)S(1)} %copy-done.6, f32[16]{0:T(128)S(1)} %add_rsqrt_fusion.1), kind=kOutput, calls=%fused_computation.50 | convolution fusion | flops 67272704 | bytes 4333632 | tf_op jit(solution)/shard_map/dot_general | solution.py:34
  91.3 0.1 reshape.236
  91.4 2.9 %fusion.41 = f32[16,1024]{1,0:T(8,128)S(1)} fusion(bf16[2048,3072]{1,0:T(8,128)(2,1)} %all-gather.2.cloned.1.call-done, bf16[16,2048]{1,0:T(8,128)(2,1)S(1)} %copy-done.3, f32[2048]{0:T(1024)S(1)} %copy-done.6, f32[16]{0:T(128)S(1)} %add_rsqrt_fusion.1), kind=kOutput, calls=%fused_computation.46 | convolution fusion | flops 67272704 | bytes 4333632 | tf_op jit(solution)/shard_map/dot_general | solution.py:34
  94.2 0.1 reshape.234
  94.3 2.9 %fusion.47 = f32[16,1024]{1,0:T(8,128)S(1)} fusion(bf16[2048,3072]{1,0:T(8,128)(2,1)} %all-gather.2.cloned.1.call-done, bf16[16,2048]{1,0:T(8,128)(2,1)S(1)} %copy-done.3, f32[2048]{0:T(1024)S(1)} %copy-done.6, f32[16]{0:T(128)S(1)} %add_rsqrt_fusion.1), kind=kOutput, calls=%fused_computation.48 | convolution fusion | flops 67272704 | bytes 4333632 | tf_op jit(solution)/shard_map/dot_general | solution.py:34
  97.3 0.7 reshape.235
  98.0 0.9 constant_dynamic-update-slice_fusion.3
  99.0 0.0 copy-start.4
  99.0 0.9 copy-done.4
  99.9 10.6 %mix.1 = (f32[16,16,64]{2,1,0:T(8,128)}, f32[16,16,4096]{2,1,0:T(8,128)}) custom-call(f32[16,6,16,64]{3,2,1,0:T(8,128)} %copy-done.4, f32[16,64]{1,0:T(8,128)} %reshape.227.gain_ref, f32[16,16,4096]{2,1,0:T(8,128)} %state_ref.1, bf16[64,4096]{1,0:T(8,128)(2,1)} %fusion.59.spread_ref, bf16[4096,64]{1,0:T(8,128)(2,1)} %fusion.20.fold_ref), custom_call_target="tpu_custom_call" | custom-call | tf_op jit(solution)/shard_map/mix/pallas_call | solution.py:115
  110.5 0.9 convert_element_type.114
  111.4 0.1 convert_element_type.115
  111.5 0.0 copy-start.9
  111.5 0.0 copy-start.7
  111.6 0.0 copy-start.8
  111.6 3.0 %multiply_reduce_fusion = (f32[16]{0:T(128)S(1)}, f32[16,2048]{1,0:T(8,128)S(1)}) fusion(bf16[16,1024]{1,0:T(8,128)(2,1)S(1)} %convert_element_type.115, bf16[1024,2048]{1,0:T(8,128)(2,1)} %param.38, bf16[16,2048]{1,0:T(8,128)(2,1)S(1)} %copy-done.3), kind=kOutput, calls=%fused_computation.78 | convolution fusion | flops 67305456 | bytes 4423744 | tf_op jit(solution)/shard_map/dot_general | solution.py:34
  114.6 0.0 copy-done.9
  114.6 0.1 multiply_convert_fusion
  114.7 0.0 copy-done.7
  114.7 2.1 convolution_bitcast_fusion
  116.8 7.8 %all-to-all-start = ((bf16[128,8,1024]{2,1,0:T(8,128)(2,1)}), bf16[128,8,1024]{2,1,0:T(8,128)(2,1)}, u32[]{:S(2)}, u32[]{:S(2)}) async-start(bf16[128,8,1024]{2,1,0:T(8,128)(2,1)} %convolution_bitcast_fusion), calls=%async_computation | async-start | bytes 4194304 | tf_op jit(solution)/shard_map/all_to_all | solution.py:217
  124.6 2.7 %fusion.121 = (bf16[512,1024]{1,0:T(8,128)(2,1)S(1)}, bf16[512,1024]{1,0:T(8,128)(2,1)}) fusion(bf16[512,2048]{1,0:T(8,128)(2,1)} %bitcast.57), kind=kLoop, calls=%fused_computation.160 | loop fusion | bytes 4194304 | tf_op jit(solution)/shard_map/slice | solution.py:246
  127.3 27.4 %all-to-all-done = bf16[128,8,1024]{2,1,0:T(8,128)(2,1)} async-done(((bf16[128,8,1024]{2,1,0:T(8,128)(2,1)}), bf16[128,8,1024]{2,1,0:T(8,128)(2,1)}, u32[]{:S(2)}, u32[]{:S(2)}) %all-to-all-start) | async-done | bytes 2097184 | tf_op jit(solution)/shard_map/all_to_all | solution.py:217
  154.7 2.4 %fusion.26 = bf16[4,128,1024]{1,2,0:T(8,128)(2,1)S(1)} fusion(bf16[4,256,1024]{2,1,0:T(8,128)(2,1)} %bitcast.1, s32[128]{0:T(128)S(1)} %get-tuple-element.21), kind=kOutput, calls=%fused_computation.35 | convolution fusion | flops 268992512 | bytes 3146240 | tf_op jit(solution)/shard_map/pq,bqc->bpc/dot_general | solution.py:232
  157.1 2.4 %fusion.25 = bf16[4,128,1024]{1,2,0:T(8,128)(2,1)S(1)} fusion(bf16[4,256,1024]{2,1,0:T(8,128)(2,1)} %bitcast.1, s32[128]{0:T(128)S(1)} %get-tuple-element.20), kind=kOutput, calls=%fused_computation.34 | convolution fusion | flops 268992512 | bytes 3146240 | tf_op jit(solution)/shard_map/pq,bqc->bpc/dot_general | solution.py:232
  159.5 1.5 pad_maximum_fusion
  161.0 4.0 %copy.40 = bf16[4,128,2048]{2,1,0:T(8,128)(2,1)} copy(bf16[4,128,2048]{1,2,0:T(8,128)(2,1)} %pad_maximum_fusion) | data formatting | bytes 4194304 | tf_op jit(solution)/shard_map/concatenate | solution.py:230
  165.0 0.0 copy-done
  165.0 3.0 %fusion.18 = f32[512,512]{1,0:T(8,128)S(1)} fusion(bf16[512,2048]{1,0:T(8,128)(2,1)} %bitcast.59, bf16[1,2048,512]{2,1,0:T(8,128)(2,1)S(1)} %copy-done), kind=kOutput, calls=%fused_computation.22 | convolution fusion | flops 1073741824 | bytes 5242880 | tf_op jit(solution)/shard_map/dot_general | solution.py:34
  168.0 1.3 fusion.30
  169.3 0.5 fusion.24
  169.8 0.5 fusion.23
  170.3 0.1 pad_maximum_fusion.1
  170.5 2.5 %copy.43 = bf16[4,256,1024]{2,1,0:T(8,128)(2,1)} copy(bf16[4,256,1024]{1,2,0:T(8,128)(2,1)S(1)} %pad_maximum_fusion.1) | data formatting | bytes 4194304 | tf_op jit(solution)/shard_map/concatenate | solution.py:245
  173.0 5.5 %convert_bitcast_fusion = bf16[128,8,1024]{2,1,0:T(8,128)(2,1)} fusion(bf16[1024,1024]{1,0:T(8,128)(2,1)} %bitcast.58, bf16[512,1024]{1,0:T(8,128)(2,1)} %get-tuple-element.11, bf16[512,1024]{1,0:T(8,128)(2,1)S(1)} %get-tuple-element.10), kind=kOutput, calls=%fused_computation.24 | convolution fusion | flops 2152726528 | bytes 6291456 | tf_op jit(solution)/shard_map/dot_general | solution.py:34
  178.5 4.5 %all-to-all-start.1 = ((bf16[128,8,1024]{2,1,0:T(8,128)(2,1)}), bf16[128,8,1024]{2,1,0:T(8,128)(2,1)S(1)}, u32[]{:S(2)}, u32[]{:S(2)}) async-start(bf16[128,8,1024]{2,1,0:T(8,128)(2,1)} %convert_bitcast_fusion), calls=%async_computation.1 | async-start | bytes 4194304 | tf_op jit(solution)/shard_map/all_to_all | solution.py:248
  183.1 2.0 fusion.124
  185.0 28.6 %all-to-all-done.1 = bf16[128,8,1024]{2,1,0:T(8,128)(2,1)S(1)} async-done(((bf16[128,8,1024]{2,1,0:T(8,128)(2,1)}), bf16[128,8,1024]{2,1,0:T(8,128)(2,1)S(1)}, u32[]{:S(2)}, u32[]{:S(2)}) %all-to-all-start.1) | async-done | bytes 2097184 | tf_op jit(solution)/shard_map/all_to_all | solution.py:248
  213.6 0.5 fusion.14
  214.2 0.0 copy-start.1
  214.2 3.7 %fusion.9 = bf16[16,2048]{1,0:T(8,128)(2,1)} fusion(f32[16,2048]{1,0:T(8,128)S(1)} %get-tuple-element.19, bf16[512,2048]{1,0:T(8,128)(2,1)} %param.42, bf16[16,2048]{1,0:T(8,128)(2,1)S(1)} %multiply_convert_fusion, bf16[2048,512]{1,0:T(8,128)(2,1)} %param.41, f32[16,1024]{1,0:T(8,128)S(1)} %get-tuple-element.13, f32[16,1024]{1,0:T(8,128)S(1)} %get-tuple-element.12, ...), kind=kOutput, calls=%fused_computation.11 | convolution fusion | flops 67289088 | bytes 4620288 | tf_op jit(solution)/shard_map/dot_general | solution.py:34
  (25 shorter events, 0.2 us)
Async XLA Ops:
  7.2 157.8 %copy-start = (bf16[1,2048,512]{2,1,0:T(8,128)(2,1)S(1)}, bf16[1,2048,512]{2,1,0:T(8,128)(2,1)}, u32[]{:S(2)}) copy-start(bf16[1,2048,512]{2,1,0:T(8,128)(2,1)} %param.43) | copy-start | bytes 6291460
  7.2 81.2 %copy-start.3 = (bf16[16,2048]{1,0:T(8,128)(2,1)S(1)}, bf16[16,2048]{1,0:T(8,128)(2,1)}, u32[]{:S(2)}) copy-start(bf16[16,2048]{1,0:T(8,128)(2,1)} %param.24) | copy-start | bytes 196612
  7.2 81.2 %copy-start.6 = (f32[2048]{0:T(1024)S(1)}, f32[2048]{0:T(1024)}, u32[]{:S(2)}) copy-start(f32[2048]{0:T(1024)} %param.26) | copy-start | bytes 24580
  7.2 81.2 %all-gather.2.cloned.1.call-start = ((), (), s32[]{:S(2)}) async-start(), calls=%async_computation.2 | async-start | bytes 12681216 | tf_op jit(solution)/shard_map/all_gather | solution.py:23
  99.0 0.9 copy-start.4
  111.5 3.0 %copy-start.9 = (f32[2048]{0:T(1024)S(1)}, f32[2048]{0:T(1024)}, u32[]{:S(2)}) copy-start(f32[2048]{0:T(1024)} %param.39) | copy-start | bytes 24580
  111.5 3.1 %copy-start.7 = (pred[16,1024]{1,0:T(8,128)(4,1)S(1)}, pred[16,1024]{1,0:T(8,128)(4,1)}, u32[]{:S(2)}) copy-start(pred[16,1024]{1,0:T(8,128)(4,1)} %get-tuple-element.7) | copy-start | bytes 49156
  111.6 3.1 %copy-start.8 = (pred[16,1024]{1,0:T(8,128)(4,1)S(1)}, pred[16,1024]{1,0:T(8,128)(4,1)}, u32[]{:S(2)}) copy-start(pred[16,1024]{1,0:T(8,128)(4,1)} %get-tuple-element.15) | copy-start | bytes 49156
  116.8 37.9 %all-to-all-start = ((bf16[128,8,1024]{2,1,0:T(8,128)(2,1)}), bf16[128,8,1024]{2,1,0:T(8,128)(2,1)}, u32[]{:S(2)}, u32[]{:S(2)}) async-start(bf16[128,8,1024]{2,1,0:T(8,128)(2,1)} %convolution_bitcast_fusion), calls=%async_computation | async-start | bytes 4194304 | tf_op jit(solution)/shard_map/all_to_all | solution.py:217
  165.0 3.0 %copy-start.2 = (bf16[4,128,2048]{2,1,0:T(8,128)(2,1)S(1)}, bf16[4,128,2048]{2,1,0:T(8,128)(2,1)}, u32[]{:S(2)}) copy-start(bf16[4,128,2048]{2,1,0:T(8,128)(2,1)} %copy.40) | copy-start | bytes 6291460
  165.0 3.0 %copy-start.10 = (bf16[1,2048,512]{2,1,0:T(8,128)(2,1)S(1)}, bf16[1,2048,512]{2,1,0:T(8,128)(2,1)}, u32[]{:S(2)}) copy-start(bf16[1,2048,512]{2,1,0:T(8,128)(2,1)} %param.44) | copy-start | bytes 6291460
  178.5 4.5 %copy-start.5 = (f32[16,1024]{1,0:T(8,128)S(1)}, f32[16,1024]{1,0:T(8,128)}, u32[]{:S(2)}) copy-start(f32[16,1024]{1,0:T(8,128)} %get-tuple-element.14) | copy-start | bytes 196612
  178.5 35.1 %all-to-all-start.1 = ((bf16[128,8,1024]{2,1,0:T(8,128)(2,1)}), bf16[128,8,1024]{2,1,0:T(8,128)(2,1)S(1)}, u32[]{:S(2)}, u32[]{:S(2)}) async-start(bf16[128,8,1024]{2,1,0:T(8,128)(2,1)} %convert_bitcast_fusion), calls=%async_computation.1 | async-start | bytes 4194304 | tf_op jit(solution)/shard_map/all_to_all | solution.py:248
  214.2 3.8 %copy-start.1 = (bf16[1,2048,512]{2,1,0:T(8,128)(2,1)S(1)}, bf16[1,2048,512]{2,1,0:T(8,128)(2,1)}, u32[]{:S(2)}) copy-start(bf16[1,2048,512]{2,1,0:T(8,128)(2,1)} %param.43) | copy-start | bytes 6291460
Sparse Core Ops, SparseCore 0:
  11.7 76.6 all-gather.1

commit v2 on v1

v2 whole, which is shorter than its diff:
```python
import jax
import jax.numpy as jnp
from jax import lax
from jax.experimental import pallas as pl
from jax.experimental.pallas import tpu as pltpu
from jax.sharding import PartitionSpec as P

HEAD = 64
MOST = 4
HALVES = 2
RING = 4
CORES = 2
GROUP = 8
LANES = 128
BLOCK = 256
NORM_EPS = 1e-06
GROUP_EPS = 0.00064
BF = jnp.bfloat16
F32 = jnp.float32


def rms_scale(inputs, gain):
    widened = inputs.astype(F32)
    return (
        widened * lax.rsqrt(jnp.mean(widened * widened, axis=-1, keepdims=True) + NORM_EPS) * gain
    )


def dot32(a, b):
    return jnp.dot(a, b, preferred_element_type=F32)


def gated_units(inputs, gate_weight, up_weight):
    return (jax.nn.silu(dot32(inputs, gate_weight)) * dot32(inputs, up_weight)).astype(BF)


def high_low(x):
    high = x.astype(BF)
    return high, (x - high.astype(F32)).astype(BF)


def iota(shape, dim):
    return lax.broadcasted_iota(jnp.int32, shape, dim)


def whole(count):
    return [pl.BlockSpec(memory_space=pltpu.VMEM) for _ in range(count)]


def mix_kernel(
    sent_ref,
    decay_ref,
    learn_ref,
    scale_ref,
    gain_ref,
    state_ref,
    spread_ref,
    fold_ref,
    output_ref,
    tokens_ref,
    second_gain_ref,
    pick_ref,
    next_ref,
    residual_ref,
    second_ref,
    chunks_ref,
):
    rows, heads, lanes = state_ref.shape
    both = rows * heads
    members = sent_ref.shape[0]
    chunk = 1024
    row = iota((both, members), 0)
    member = iota((both, members), 1)
    mine = ((row // heads) == (member % rows)) & ((row % heads) // CORES == member // rows)
    owned = dot32(mine.astype(BF), sent_ref[...])
    side = (iota((both, LANES), 0) % CORES) == (iota((both, LANES), 1) // HEAD)
    first_half = iota((both, LANES), 1) < HEAD

    def part(i):
        return jnp.where(side, owned[:, i * LANES : (i + 1) * LANES], 0.0)

    def twice(x):
        return x + pltpu.roll(x, HEAD, 1)

    reader2 = twice(part(0))
    key2 = twice(part(1))
    value = part(2).astype(BF)
    decay2 = decay_ref[...]
    scaled = key2 * scale_ref[...]
    total = jnp.sum(scaled * scaled, axis=-1, keepdims=True) * 0.5
    dir2 = scaled / jnp.sqrt(total + 1.0)
    taken2 = dir2 * learn_ref[...]

    removed2 = jnp.zeros((both, LANES), F32)
    for c in range(lanes // chunk):
        pieces = []
        for j in range(chunk // LANES):
            at = c * chunk + j * LANES
            state = state_ref[:, :, at : at + LANES].reshape(both, LANES)
            pieces.append((state * dir2).astype(BF))
        removed2 = removed2 + dot32(
            jnp.concatenate(pieces, axis=1), fold_ref[c * chunk : (c + 1) * chunk, :]
        )
    high, low = high_low(removed2)
    known = jnp.where(first_half, high.astype(F32), low.astype(F32)).astype(BF)
    readout2 = jnp.zeros((both, LANES), F32)
    for c in range(lanes // chunk):
        spread = spread_ref[:, c * chunk : (c + 1) * chunk]
        removed_wide = dot32(known, spread)
        value_wide = dot32(value, spread)
        pieces = []
        for j in range(chunk // LANES):
            at = c * chunk + j * LANES
            sub = slice(j * LANES, (j + 1) * LANES)
            state = (
                state_ref[:, :, at : at + LANES].reshape(both, LANES) * decay2
                - removed_wide[:, sub] * taken2
                + value_wide[:, sub] * key2
            )
            next_ref[:, :, at : at + LANES] = state.reshape(rows, heads, LANES)
            pieces.append((state * reader2).astype(BF))
        readout2 = readout2 + dot32(
            jnp.concatenate(pieces, axis=1), fold_ref[c * chunk : (c + 1) * chunk, :]
        )
    centre = jnp.mean(readout2, axis=-1, keepdims=True)
    apart = readout2 - centre
    spread_of = jnp.mean(apart * apart, axis=-1, keepdims=True)
    mixed2 = apart * lax.rsqrt(spread_of + GROUP_EPS) * gain_ref[...]

    width = heads * HEAD
    own_head = (iota((both, width), 0) % heads) == (iota((both, width), 1) // HEAD)
    laid = jnp.where(own_head, jnp.concatenate([mixed2] * (width // LANES), axis=1), 0.0)
    collect = (iota((rows, both), 0) == iota((rows, both), 1) // heads).astype(BF)
    mixed = dot32(collect, laid.astype(BF)).astype(BF)
    residual = (tokens_ref[...].astype(F32) + dot32(mixed, output_ref[...])).astype(BF)
    second = rms_scale(residual, second_gain_ref[...]).astype(BF)
    residual_ref[...] = residual
    second_ref[...] = second
    half = second.shape[1] // HALVES
    halves = jnp.concatenate([second[:, h * half : (h + 1) * half] for h in range(HALVES)], axis=0)
    chunks_ref[...] = dot32(pick_ref[...], halves).astype(BF)


def mix_heads(sent, decay, learn, scale, gain, state_old, w_output, tokens, second_gain, pick):
    rows, heads, lanes = state_old.shape
    width = tokens.shape[1]
    lane = jnp.arange(lanes, dtype=jnp.int32)
    entry = jnp.arange(LANES, dtype=jnp.int32) % HEAD
    spread = (entry[:, None] == lane[None, :] // HEAD).astype(BF)
    fold = (lane[:, None] // HEAD == entry[None, :]).astype(BF)
    return pl.pallas_call(
        mix_kernel,
        in_specs=whole(12),
        out_specs=whole(4),
        out_shape=[
            jax.ShapeDtypeStruct(state_old.shape, F32),
            jax.ShapeDtypeStruct((rows, width), BF),
            jax.ShapeDtypeStruct((rows, width), BF),
            jax.ShapeDtypeStruct((pick.shape[0], width // HALVES), BF),
        ],
        name="mix",
    )(
        sent,
        decay,
        learn,
        scale,
        gain,
        state_old,
        spread,
        fold,
        w_output,
        tokens,
        second_gain[None, :],
        pick,
    )


def expert_kernel(chunks_ref, gate_ref, up_ref, down_ref, out_ref):
    half = chunks_ref.shape[1]
    kept = BLOCK // HALVES
    row = iota((BLOCK, BLOCK), 0)
    column = iota((BLOCK, BLOCK), 1)
    slot = row % kept
    split = (column == slot // MOST * (MOST * HALVES) + row // kept * MOST + slot % MOST).astype(BF)
    back = iota((BLOCK, BLOCK), 1)
    back_slot = back % kept
    source = back_slot // MOST * (MOST * HALVES) + back // kept * MOST + back_slot % MOST
    join = (iota((BLOCK, BLOCK), 0) == source).astype(BF)
    inputs = []
    for b in range(chunks_ref.shape[0] // BLOCK):
        apart = dot32(split, chunks_ref[b * BLOCK : (b + 1) * BLOCK, :]).astype(BF)
        inputs.append(jnp.concatenate([apart[:kept], apart[kept:]], axis=1))
    inputs = jnp.concatenate(inputs, axis=0)
    hidden = gated_units(inputs, gate_ref[...], up_ref[...])
    result = dot32(hidden, down_ref[...]).astype(BF)
    for b in range(chunks_ref.shape[0] // BLOCK):
        mine = result[b * kept : (b + 1) * kept]
        stacked = jnp.concatenate([mine[:, :half], mine[:, half:]], axis=0)
        out_ref[b * BLOCK : (b + 1) * BLOCK, :] = dot32(join, stacked).astype(BF)


def run_expert(chunks, gate, up, down):
    return pl.pallas_call(
        expert_kernel,
        in_specs=whole(4),
        out_specs=whole(1)[0],
        out_shape=jax.ShapeDtypeStruct(chunks.shape, BF),
        name="expert",
    )(chunks, gate, up, down)


def combine_kernel(weigh_ref, returned_ref, residual_ref, shared_ref, out_ref):
    rows = residual_ref.shape[0]
    half = returned_ref.shape[1]
    parts = dot32(weigh_ref[...], returned_ref[...])
    parts = parts[: HALVES * rows] + parts[HALVES * rows :]
    for h in range(HALVES):
        at = slice(h * half, (h + 1) * half)
        out_ref[:, at] = (
            residual_ref[:, at].astype(F32)
            + shared_ref[:, at]
            + parts[h * rows : (h + 1) * rows]
        ).astype(BF)


def combine(weigh, returned, residual, shared):
    return pl.pallas_call(
        combine_kernel,
        in_specs=whole(4),
        out_specs=whole(1)[0],
        out_shape=jax.ShapeDtypeStruct(residual.shape, BF),
        name="combine",
    )(weigh, returned, residual, shared)


def exchanged(x, groups=None):
    return lax.all_to_all(
        x, "ep", split_axis=0, concat_axis=0, tiled=True, axis_index_groups=groups
    )


def gathered_rows(normed, devices, me):
    rows, width = normed.shape
    core = me % CORES
    place = me // CORES % RING
    other = lax.ppermute(normed, "ep", [(d, d ^ 1) for d in range(devices)])
    pair = jnp.where(
        core == 0, jnp.stack([normed, other], axis=0), jnp.stack([other, normed], axis=0)
    )
    held = jnp.zeros((RING, CORES, rows, width), BF)
    held = lax.dynamic_update_slice(held, pair[None], (place, 0, 0, 0))
    for step in range(1, RING):
        hop = [
            (d, d // GROUP * GROUP + (d % GROUP + CORES * step) % GROUP) for d in range(devices)
        ]
        moved = lax.ppermute(pair, "ep", hop)
        held = lax.dynamic_update_slice(held, moved[None], ((place - step) % RING, 0, 0, 0))
    return held.reshape(GROUP * rows, width)


def per_device(
    tokens,
    recurrent_state,
    first_gain,
    w_receptance,
    w_key,
    w_value,
    decay_down,
    decay_up,
    decay_base,
    rate_down,
    rate_up,
    rate_base,
    key_scale,
    head_gain,
    w_output,
    second_gain,
    shared_gate,
    shared_up,
    shared_down,
    expert_gate,
    expert_up,
    expert_down,
    routes,
    route_weights,
):
    rows, width = tokens.shape
    heads = recurrent_state.shape[1]
    half = width // HALVES
    devices = lax.axis_size("ep")
    me = lax.axis_index("ep")

    columns = jnp.stack([w_receptance, w_key, w_value], axis=1).reshape(rows, 3, GROUP, LANES)
    columns = columns.transpose(2, 0, 1, 3).reshape(1, GROUP, rows, 3 * LANES)
    columns = jnp.broadcast_to(columns, (devices // GROUP,) + columns.shape[1:])
    weights = exchanged(columns.reshape(devices, rows, 3 * LANES)).reshape(width, 3 * LANES)
    normed = rms_scale(tokens, first_gain).astype(BF)
    group_rows = gathered_rows(normed, devices, me)

    own_routes = lax.dynamic_slice_in_dim(routes, me * rows, rows, 0)
    own_weights = lax.dynamic_slice_in_dim(route_weights, me * rows, rows, 0)
    place = jnp.arange(devices * MOST * HALVES, dtype=jnp.int32)
    named = own_routes[:, :, None] == (place // (MOST * HALVES))[None, None, :]
    weight = jnp.sum(jnp.where(named, own_weights[:, :, None], 0.0), axis=1)
    named = jnp.any(named, axis=1)
    order = jnp.arange(rows, dtype=jnp.int32)
    before = (order[None, :] < order[:, None]).astype(BF)
    slot = dot32(before, named.astype(BF))
    chosen = named & (slot == (place % MOST)[None, :].astype(F32))
    side = (place // MOST) % HALVES
    picks = [chosen & (side == h)[None, :] for h in range(HALVES)]
    pick = jnp.concatenate(picks, axis=0).astype(BF).T
    weigh_high, weigh_low = high_low(
        jnp.concatenate([jnp.where(p, weight, 0.0) for p in picks], axis=0)
    )
    weigh = jnp.concatenate([weigh_high, weigh_low], axis=0)

    decay_low = jnp.tanh(dot32(normed, decay_down)).astype(BF)
    decay_pre = decay_base + dot32(decay_low, decay_up)
    decay_rate = jnp.exp(-jnp.exp(-jax.nn.softplus(-decay_pre) - 0.5))
    rate_low = dot32(normed, rate_down).astype(BF)
    learn_rate = jax.nn.sigmoid(rate_base + dot32(rate_low, rate_up))

    def by_head(x):
        x = jnp.broadcast_to(x, (rows, heads * HEAD)).reshape(rows * heads, HEAD)
        return jnp.concatenate([x, x], axis=1)

    sums = dot32(group_rows, weights).astype(BF)
    around = [
        list(range(first, first + GROUP)) for first in range(0, devices, GROUP)
    ]
    sent = exchanged(sums.reshape(GROUP, rows, 3 * LANES), around)
    new_state, residual, second, outgoing = mix_heads(
        sent.reshape(GROUP * rows, 3 * LANES),
        by_head(decay_rate),
        by_head(learn_rate),
        by_head(key_scale),
        by_head(head_gain),
        recurrent_state,
        w_output,
        tokens,
        second_gain,
        pick,
    )
    received = exchanged(outgoing.reshape(devices, MOST * HALVES, half))
    shared = dot32(gated_units(second, shared_gate, shared_up), shared_down)
    produced = run_expert(
        received.reshape(devices * MOST * HALVES, half),
        expert_gate[0],
        expert_up[0],
        expert_down[0],
    )
    returned = exchanged(produced.reshape(devices, MOST * HALVES, half))
    new_tokens = combine(
        weigh, returned.reshape(devices * MOST * HALVES, half), residual, shared
    )
    return (new_tokens, new_state)


def solution(mesh):
    row = P("ep", None)
    block = P("ep", None, None)
    copied = P()
    in_specs = (
        (row, block, copied, row, row, row)
        + (copied,) * 13
        + (block, block, block, copied, copied)
    )
    return jax.shard_map(
        per_device, mesh=mesh, in_specs=in_specs, out_specs=(row, block), check_vma=False
    )
```

time: 226 us -> 154 us (0.68)
  waiting for transfers between devices: 123 us -> 41.3 us
  blocking collectives: 0 us -> 36 us
  matrix products: 39.3 us -> 8.35 us
  starting transfers between devices: 12.4 us -> 27.6 us
  between operations: 14.4 us -> 1.09 us
  Pallas kernels: 10.6 us -> 22.7 us
  local copies, waits for them, and re-layouts: 16 us -> 7.37 us
    all_gather x1 -> x0, waiting for transfers between devices: 67.1 us -> none  [sent_together(): lax.all_gather(both, axis, axis=dim, tiled=True)]
    all_to_all x0 -> x1, blocking collectives: none -> 36 us  [exchanged(): lax.all_to_all(x, 'ep', split_axis=0, concat_axis=0, tiled=True, axis_ind...]
    all_to_all x2 -> x3, waiting for transfers between devices: 56 us -> 29.5 us  [exchanged(): lax.all_to_all(x, 'ep', split_axis=0, concat_axis=0, tiled=True, axis_ind...]
    dot_general x13 -> x6, matrix products: 31.5 us -> 8.35 us  [dot32(): return jnp.dot(a, b, preferred_element_type=F32)]
    pallas_call x1 -> x3, Pallas kernels: 10.6 us -> 22.7 us  [the longest x1 10.7 us: mix_heads(): pl.pallas_call(mix_kernel, in_specs=whole(12), out_specs=whole(4), out_sh...]
    ppermute x0 -> x4, waiting for transfers between devices: none -> 11.8 us  [the longest x3 11.8 us: gathered_rows(): moved = lax.ppermute(pair, 'ep', hop)]
    all_to_all x2 -> x3, starting transfers between devices: 12.4 us -> 22.4 us  [exchanged(): lax.all_to_all(x, 'ep', split_axis=0, concat_axis=0, tiled=True, axis_ind...]
    dot_general x5 -> x0, matrix products: 7.87 us -> none  [the longest x2 4.78 us: per_device(): jnp.einsum('pq,bqc->bpc', u, chunks, preferred_element_type=F32).astype(BF)]
  transfers between devices with their start and end apart: 3 -> 7, of which waited for: 3 -> 4; matrix products, arithmetic and copies ran while one was open for 8% -> 13% of each run, Pallas kernels for 0% -> 0%
where the time goes in v2:
time: 154 us; the launch traced here: 153 us
  waiting for transfers between devices  41.3 us (27%)
  blocking collectives  36 us (23%)
  starting transfers between devices  27.6 us (18%)
  Pallas kernels  22.7 us (15%)
  other arithmetic  9.03 us (6%)
  matrix products  8.35 us (5%)
  local copies, waits for them, and re-layouts  7.37 us (5%)
    all_to_all x1, blocking collectives, exchanged(): lax.all_to_all(x, 'ep', split_axis=0, concat_axis=0, tiled=True, axis_ind...  36 us
    all_to_all x3, waiting for transfers between devices, exchanged(): lax.all_to_all(x, 'ep', split_axis=0, concat_axis=0, tiled=True, axis_ind...  29.5 us
    all_to_all x3, starting transfers between devices, exchanged(): lax.all_to_all(x, 'ep', split_axis=0, concat_axis=0, tiled=True, axis_ind...  22.4 us
    ppermute x3, waiting for transfers between devices, gathered_rows(): moved = lax.ppermute(pair, 'ep', hop)  11.8 us
    pallas_call x1, Pallas kernels, mix_heads(): pl.pallas_call(mix_kernel, in_specs=whole(12), out_specs=whole(4), out_sh...  10.7 us
    pallas_call x1, Pallas kernels, run_expert(): pl.pallas_call(expert_kernel, in_specs=whole(4), out_specs=whole(1)[0], o...  9.3 us
    dot_general x6, matrix products, dot32(): return jnp.dot(a, b, preferred_element_type=F32)  8.35 us
    ppermute x3, starting transfers between devices, gathered_rows(): moved = lax.ppermute(pair, 'ep', hop)  3.79 us
  transfers between devices with their start and end apart: 7, of which 4 were waited for; matrix products, arithmetic and copies ran while one was open for 13% of the time, Pallas kernels for 0%

profile of v2, /device:TPU:1, one launch (start us, length us, event | category | flops | bytes accessed | tf_op | source)
XLA Modules:
  0.0 153.5 jit_solution(1703731602684657638)
XLA Ops:
  0.6 0.0 copy-start
  0.6 1.1 fusion.10
  1.8 0.9 fusion.12
  2.7 1.5 collective-permute-start
  4.2 0.8 copy.39
  4.9 0.1 copy.35
  5.0 0.8 copy.40
  5.8 0.1 copy.36
  5.8 0.8 copy.41
  6.6 0.1 copy.37
  6.6 0.2 maximum_bitcast_fusion
  6.9 0.1 broadcast_in_dim.77
  7.0 0.0 copy-start.1
  7.0 0.0 copy-start.6
  7.0 1.3 broadcast_in_dim.78
  8.3 10.6 %all-to-all-start = ((bf16[128,16,384]{2,1,0:T(8,128)(2,1)}), bf16[128,16,384]{2,1,0:T(8,128)(2,1)}, u32[]{:S(2)}, u32[]{:S(2)}) async-start(bf16[128,16,384]{2,1,0:T(8,128)(2,1)} %bitcast.59), calls=%async_computation | async-start | bytes 3145728 | tf_op jit(solution)/shard_map/all_to_all | solution.py:237
  19.0 0.0 copy-start.9
  19.0 0.0 copy-start.10
  19.0 0.0 copy-start.11
  19.0 0.0 copy-start.12
  19.0 0.0 copy-start.4
  19.0 0.0 copy-start.5
  19.0 0.0 copy-start.7
  19.2 0.0 copy-done.1
  19.2 0.0 copy-done.6
  19.2 0.1 fusion.56
  19.3 0.1 fusion.55
  19.4 2.7 %compare_convert_fusion.fold_ref = bf16[4096,128]{1,0:T(8,128)(2,1)} fusion(s32[128]{0:T(128)S(1)} %and_select_fusion, s32[4096]{0:T(1024)S(1)} %add_select_fusion), kind=kLoop, calls=%fused_computation | loop fusion | flops 1048576 | bytes 1065472 | tf_op jit(solution)/shard_map/convert_element_type | solution.py:150
  22.1 1.2 compare_convert_fusion.1.spread_ref
  23.3 0.8 constant_dynamic-slice_fusion.1
  24.1 0.8 constant_dynamic-slice_fusion
  24.8 0.1 broadcast_in_dim.79
  24.9 0.1 broadcast_in_dim.82
  25.0 0.1 compare_reduce_fusion
  25.1 0.1 fusion.9
  25.2 0.4 fusion.3
  25.6 0.1 reshape.274
  25.7 0.4 fusion.20
  26.1 0.1 reshape.273
  26.2 0.2 broadcast_select_fusion.1
  26.4 0.9 copy.38.pick_ref
  27.2 0.8 pad_maximum_fusion.2
  28.1 0.0 collective-permute-done
  28.1 2.6 %collective-permute-start.3 = (bf16[2,16,2048]{2,1,0:T(8,128)(2,1)S(1)}, bf16[2,16,2048]{2,1,0:T(8,128)(2,1)S(1)}, u32[]{:S(2)}, u32[]{:S(2)}) collective-permute-start(bf16[2,16,2048]{2,1,0:T(8,128)(2,1)S(1)} %maximum_select_fusion.1), channel_id=1, source_target_pairs={{0,6},{1,7},{2,0},{3,1},{4,2},{5,3},{6,4},{7,5},{8,14},{9,15},{10,... | collective-permute-start | bytes 393224 | tf_op jit(solution)/shard_map/ppermute | solution.py:256
  30.7 0.6 collective-permute-start.2
  31.3 0.6 collective-permute-start.1
  31.9 11.8 %collective-permute-done.1 = bf16[2,16,2048]{2,1,0:T(8,128)(2,1)S(1)} collective-permute-done((bf16[2,16,2048]{2,1,0:T(8,128)(2,1)S(1)}, bf16[2,16,2048]{2,1,0:T(8,128)(2,1)S(1)}, u32[]{:S(2)}, u32[]{:S(2)}) %collective-permute-start.1) | collective-permute-done | bytes 131104 | tf_op jit(solution)/shard_map/ppermute | solution.py:256
  43.7 0.0 collective-permute-done.2
  43.8 0.0 collective-permute-done.3
  43.8 0.8 all-to-all-done
  44.6 2.5 %convolution_convert_fusion = bf16[128,384]{1,0:T(8,128)(2,1)} fusion(bf16[128,2048]{1,0:T(8,128)(2,1)S(1)} %bitcast.64, bf16[2048,384]{1,0:T(8,128)(2,1)} %bitcast.10), kind=kOutput, calls=%fused_computation.2 | convolution fusion | flops 201375744 | bytes 2195456 | tf_op jit(solution)/shard_map/dot_general | solution.py:30
  47.1 6.2 %all-to-all-start.1 = ((bf16[8,16,384]{2,1,0:T(8,128)(2,1)}), bf16[8,16,384]{2,1,0:T(8,128)(2,1)S(1)}, u32[]{:S(2)}, u32[]{:S(2)}) async-start(bf16[8,16,384]{2,1,0:T(8,128)(2,1)} %bitcast.11), calls=%async_computation.1 | async-start | bytes 196608 | tf_op jit(solution)/shard_map/all_to_all | solution.py:237
  53.3 0.8 pad_maximum_fusion.4
  54.1 4.1 %all-to-all-done.1 = bf16[8,16,384]{2,1,0:T(8,128)(2,1)S(1)} async-done(((bf16[8,16,384]{2,1,0:T(8,128)(2,1)}), bf16[8,16,384]{2,1,0:T(8,128)(2,1)S(1)}, u32[]{:S(2)}, u32[]{:S(2)}) %all-to-all-start.1) | async-done | bytes 98336 | tf_op jit(solution)/shard_map/all_to_all | solution.py:237
  58.3 0.6 copy-done.2
  58.9 10.7 %mix.1 = (f32[16,16,4096]{2,1,0:T(8,128)}, bf16[16,2048]{1,0:T(8,128)(2,1)}, bf16[16,2048]{1,0:T(8,128)(2,1)}, bf16[1024,1024]{1,0:T(8,128)(2,1)}) custom-call(bf16[128,384]{1,0:T(8,128)(2,1)} %bitcast.67, f32[256,128]{1,0:T(8,128)} %get-tuple-element.18.decay_ref, f32[256,128]{1,0:T(8,128)} %get-tuple-element.19.learn_ref, ...), custom_call_target="tpu_custom_call" | custom-call | tf_op jit(solution)/shard_map/mix/pallas_call | solution.py:151
  69.6 36.0 %all_to_all.20 = bf16[128,8,1024]{2,1,0:T(8,128)(2,1)} all-to-all(bf16[128,8,1024]{2,1,0:T(8,128)(2,1)} %bitcast.63), channel_id=1, replica_groups=mesh['ep'=128] {'ep'}, dimensions={0} | all-to-all | bytes 4194304 | tf_op jit(solution)/shard_map/all_to_all | solution.py:237
  105.6 9.3 %expert.1 = bf16[1024,1024]{1,0:T(8,128)(2,1)} custom-call(bf16[1024,1024]{1,0:T(8,128)(2,1)} %bitcast.58, bf16[2048,512]{1,0:T(8,128)(2,1)} %bitcast.60, bf16[2048,512]{1,0:T(8,128)(2,1)} %bitcast.61, bf16[512,2048]{1,0:T(8,128)(2,1)} %bitcast.62), custom_call_target="tpu_custom_call" | custom-call | tf_op jit(solution)/shard_map/expert/pallas_call | solution.py:203
  114.9 5.6 %all-to-all-start.3 = ((bf16[128,8,1024]{2,1,0:T(8,128)(2,1)}), bf16[128,8,1024]{2,1,0:T(8,128)(2,1)}, u32[]{:S(2)}, u32[]{:S(2)}) async-start(bf16[128,8,1024]{2,1,0:T(8,128)(2,1)} %bitcast.57), calls=%async_computation.3 | async-start | bytes 4194304 | tf_op jit(solution)/shard_map/all_to_all | solution.py:237
  120.5 0.7 pad_maximum_fusion.1.weigh_ref
  121.2 2.0 %fusion.40 = f32[16,512]{1,0:T(8,128)S(1)} fusion(bf16[16,2048]{1,0:T(8,128)(2,1)S(1)} %copy-done.3, bf16[2048,512]{1,0:T(8,128)(2,1)} %param.40), kind=kOutput, calls=%fused_computation.93 | convolution fusion | flops 33554432 | bytes 2195456 | tf_op jit(solution)/shard_map/dot_general | solution.py:30
  123.2 3.0 %fusion.7.shared_ref = f32[16,2048]{1,0:T(8,128)} fusion(bf16[512,2048]{1,0:T(8,128)(2,1)S(1)} %copy-done, bf16[16,2048]{1,0:T(8,128)(2,1)S(1)} %copy-done.3, bf16[2048,512]{1,0:T(8,128)(2,1)} %param.41, f32[16,512]{1,0:T(8,128)S(1)} %fusion.40), kind=kOutput, calls=%fused_computation.14 | convolution fusion | flops 67158016 | bytes 4423680 | tf_op jit(solution)/shard_map/dot_general | solution.py:30
  126.2 24.6 %all-to-all-done.3 = bf16[128,8,1024]{2,1,0:T(8,128)(2,1)} async-done(((bf16[128,8,1024]{2,1,0:T(8,128)(2,1)}), bf16[128,8,1024]{2,1,0:T(8,128)(2,1)}, u32[]{:S(2)}, u32[]{:S(2)}) %all-to-all-start.3) | async-done | bytes 2097184 | tf_op jit(solution)/shard_map/all_to_all | solution.py:237
  150.8 2.7 %combine.1 = bf16[16,2048]{1,0:T(8,128)(2,1)} custom-call(bf16[64,1024]{1,0:T(8,128)(2,1)} %pad_maximum_fusion.1.weigh_ref, bf16[1024,1024]{1,0:T(8,128)(2,1)} %bitcast.23.returned_ref, bf16[16,2048]{1,0:T(8,128)(2,1)} %get-tuple-element.7.residual_ref, f32[16,2048]{1,0:T(8,128)} %fusion.7.shared_ref), custom_call_target="tpu_custom_call" | custom-call | tf_op jit(solution)/shard_map/combine/pallas_call | solution.py:227
  (30 shorter events, 0.2 us)
Async XLA Ops:
  0.6 122.5 %copy-start = (bf16[512,2048]{1,0:T(8,128)(2,1)S(1)}, bf16[512,2048]{1,0:T(8,128)(2,1)}, u32[]{:S(2)}) copy-start(bf16[512,2048]{1,0:T(8,128)(2,1)} %param.42) | copy-start | bytes 6291460
  2.7 25.3 %collective-permute-start = (bf16[16,2048]{1,0:T(8,128)(2,1)S(1)}, bf16[16,2048]{1,0:T(8,128)(2,1)S(1)}, u32[]{:S(2)}, u32[]{:S(2)}) collective-permute-start(bf16[16,2048]{1,0:T(8,128)(2,1)S(1)} %fusion.12), channel_id=1, source_target_pairs={{0,1},{1,0},{2,3},{3,2},{4,5},{5,4},{6,7},{7,6},{8,9},{9,8},{10,11... | collective-permute-start | bytes 196616 | tf_op jit(solution)/shard_map/ppermute | solution.py:246
  7.0 12.2 %copy-start.1 = (bf16[16,2048]{1,0:T(8,128)(2,1)S(1)}, bf16[16,2048]{1,0:T(8,128)(2,1)}, u32[]{:S(2)}) copy-start(bf16[16,2048]{1,0:T(8,128)(2,1)} %tokens_ref.1) | copy-start | bytes 196612
  7.0 12.2 %copy-start.6 = (f32[2048]{0:T(1024)S(1)}, f32[2048]{0:T(1024)}, u32[]{:S(2)}) copy-start(f32[2048]{0:T(1024)} %param.26) | copy-start | bytes 24580
  8.3 16.5 %copy-start.8 = (f32[1024]{0:T(1024)S(1)}, f32[1024]{0:T(1024)}, u32[]{:S(2)}) copy-start(f32[1024]{0:T(1024)} %param.36) | copy-start | bytes 12292
  8.3 36.3 %all-to-all-start = ((bf16[128,16,384]{2,1,0:T(8,128)(2,1)}), bf16[128,16,384]{2,1,0:T(8,128)(2,1)}, u32[]{:S(2)}, u32[]{:S(2)}) async-start(bf16[128,16,384]{2,1,0:T(8,128)(2,1)} %bitcast.59), calls=%async_computation | async-start | bytes 3145728 | tf_op jit(solution)/shard_map/all_to_all | solution.py:237
  19.0 5.9 %copy-start.9 = (f32[1024]{0:T(1024)S(1)}, f32[1024]{0:T(1024)}, u32[]{:S(2)}) copy-start(f32[1024]{0:T(1024)} %param.37) | copy-start | bytes 12292
  19.0 6.2 %copy-start.10 = (bf16[2048,64]{0,1:T(8,128)(2,1)S(1)}, bf16[2048,64]{0,1:T(8,128)(2,1)}, u32[]{:S(2)}) copy-start(bf16[2048,64]{0,1:T(8,128)(2,1)} %param.33) | copy-start | bytes 786436
  19.0 6.2 %copy-start.11 = (bf16[64,1024]{1,0:T(8,128)(2,1)S(1)}, bf16[64,1024]{1,0:T(8,128)(2,1)}, u32[]{:S(2)}) copy-start(bf16[64,1024]{1,0:T(8,128)(2,1)} %param.34) | copy-start | bytes 393220
  19.0 6.2 %copy-start.12 = (f32[1024]{0:T(1024)S(1)}, f32[1024]{0:T(1024)}, u32[]{:S(2)}) copy-start(f32[1024]{0:T(1024)} %param.35) | copy-start | bytes 12292
  19.0 6.7 %copy-start.4 = (bf16[2048,64]{0,1:T(8,128)(2,1)S(1)}, bf16[2048,64]{0,1:T(8,128)(2,1)}, u32[]{:S(2)}) copy-start(bf16[2048,64]{0,1:T(8,128)(2,1)} %param.30) | copy-start | bytes 786436
  19.0 6.6 %copy-start.5 = (bf16[64,1024]{1,0:T(8,128)(2,1)S(1)}, bf16[64,1024]{1,0:T(8,128)(2,1)}, u32[]{:S(2)}) copy-start(bf16[64,1024]{1,0:T(8,128)(2,1)} %param.31) | copy-start | bytes 393220
  19.0 6.6 %copy-start.7 = (f32[1024]{0:T(1024)S(1)}, f32[1024]{0:T(1024)}, u32[]{:S(2)}) copy-start(f32[1024]{0:T(1024)} %param.32) | copy-start | bytes 12292
  28.1 15.7 %collective-permute-start.3 = (bf16[2,16,2048]{2,1,0:T(8,128)(2,1)S(1)}, bf16[2,16,2048]{2,1,0:T(8,128)(2,1)S(1)}, u32[]{:S(2)}, u32[]{:S(2)}) collective-permute-start(bf16[2,16,2048]{2,1,0:T(8,128)(2,1)S(1)} %maximum_select_fusion.1), channel_id=1, source_target_pairs={{0,6},{1,7},{2,0},{3,1},{4,2},{5,3},{6,4},{7,5},{8,14},{9,15},{10,... | collective-permute-start | bytes 393224 | tf_op jit(solution)/shard_map/ppermute | solution.py:256
  30.7 13.0 %collective-permute-start.2 = (bf16[2,16,2048]{2,1,0:T(8,128)(2,1)S(1)}, bf16[2,16,2048]{2,1,0:T(8,128)(2,1)S(1)}, u32[]{:S(2)}, u32[]{:S(2)}) collective-permute-start(bf16[2,16,2048]{2,1,0:T(8,128)(2,1)S(1)} %maximum_select_fusion.1), channel_id=1, source_target_pairs={{0,4},{1,5},{2,6},{3,7},{4,0},{5,1},{6,2},{7,3},{8,12},{9,13},{10,... | collective-permute-start | bytes 393224 | tf_op jit(solution)/shard_map/ppermute | solution.py:256
  31.3 12.4 %collective-permute-start.1 = (bf16[2,16,2048]{2,1,0:T(8,128)(2,1)S(1)}, bf16[2,16,2048]{2,1,0:T(8,128)(2,1)S(1)}, u32[]{:S(2)}, u32[]{:S(2)}) collective-permute-start(bf16[2,16,2048]{2,1,0:T(8,128)(2,1)S(1)} %maximum_select_fusion.1), channel_id=1, source_target_pairs={{0,2},{1,3},{2,4},{3,5},{4,6},{5,7},{6,0},{7,1},{8,10},{9,11},{10,... | collective-permute-start | bytes 393224 | tf_op jit(solution)/shard_map/ppermute | solution.py:256
  47.1 11.2 %all-to-all-start.1 = ((bf16[8,16,384]{2,1,0:T(8,128)(2,1)}), bf16[8,16,384]{2,1,0:T(8,128)(2,1)S(1)}, u32[]{:S(2)}, u32[]{:S(2)}) async-start(bf16[8,16,384]{2,1,0:T(8,128)(2,1)} %bitcast.11), calls=%async_computation.1 | async-start | bytes 196608 | tf_op jit(solution)/shard_map/all_to_all | solution.py:237
  58.3 0.6 copy-start.2
  114.9 6.3 %copy-start.3 = (bf16[16,2048]{1,0:T(8,128)(2,1)S(1)}, bf16[16,2048]{1,0:T(8,128)(2,1)}, u32[]{:S(2)}) copy-start(bf16[16,2048]{1,0:T(8,128)(2,1)} %get-tuple-element.8) | copy-start | bytes 196612
  114.9 35.9 %all-to-all-start.3 = ((bf16[128,8,1024]{2,1,0:T(8,128)(2,1)}), bf16[128,8,1024]{2,1,0:T(8,128)(2,1)}, u32[]{:S(2)}, u32[]{:S(2)}) async-start(bf16[128,8,1024]{2,1,0:T(8,128)(2,1)} %bitcast.57), calls=%async_computation.3 | async-start | bytes 4194304 | tf_op jit(solution)/shard_map/all_to_all | solution.py:237

commit v3 on v2

v3 whole, which is shorter than its diff:
```python
import jax
import jax.numpy as jnp
from jax import lax
from jax.experimental import pallas as pl
from jax.experimental.pallas import tpu as pltpu
from jax.sharding import PartitionSpec as P

HEAD = 64
MOST = 4
HALVES = 2
RING = 4
CORES = 2
GROUP = 8
PLANES = 4
LANES = 128
BLOCK = 256
COLUMN = 1024
NORM_EPS = 1e-06
GROUP_EPS = 0.00064
BF = jnp.bfloat16
F32 = jnp.float32


def rms_scale(inputs, gain):
    widened = inputs.astype(F32)
    return (
        widened * lax.rsqrt(jnp.mean(widened * widened, axis=-1, keepdims=True) + NORM_EPS) * gain
    )


def dot32(a, b):
    return jnp.dot(a, b, preferred_element_type=F32)


def gated_units(inputs, gate_weight, up_weight):
    return (jax.nn.silu(dot32(inputs, gate_weight)) * dot32(inputs, up_weight)).astype(BF)


def high_low(x):
    high = x.astype(BF)
    return high, (x - high.astype(F32)).astype(BF)


def iota(shape, dim):
    return lax.broadcasted_iota(jnp.int32, shape, dim)


def whole(count):
    return [pl.BlockSpec(memory_space=pltpu.VMEM) for _ in range(count)]


def in_hbm(x):
    return pltpu.with_memory_space_constraint(x, pltpu.HBM)


def room(mib):
    return pltpu.CompilerParams(vmem_limit_bytes=mib * 2**20)


def fold_matrix(column):
    value = iota((COLUMN, LANES), 0) // HEAD + column * (COLUMN // HEAD)
    return (value == iota((COLUMN, LANES), 1) % HEAD).astype(BF)


def spread_matrix(column):
    value = iota((LANES, COLUMN), 1) // HEAD + column * (COLUMN // HEAD)
    return (value == iota((LANES, COLUMN), 0) % HEAD).astype(BF)


def prepare_kernel(
    routes_ref,
    weights_ref,
    tokens_ref,
    first_gain_ref,
    decay_down_ref,
    decay_up_ref,
    decay_base_ref,
    rate_down_ref,
    rate_up_ref,
    rate_base_ref,
    scale_ref,
    gain_ref,
    pick_ref,
    weigh_ref,
    decay_out,
    learn_out,
    scale_out,
    gain_out,
):
    rows, choices = routes_ref.shape
    total = pick_ref.shape[1]
    place = iota((rows, total), 1)
    named = jnp.zeros((rows, total), F32)
    weight = jnp.zeros((rows, total), F32)
    for j in range(choices):
        match = routes_ref[:, j : j + 1] == place // (MOST * HALVES)
        named = jnp.where(match, 1.0, named)
        weight = jnp.where(match, weights_ref[:, j : j + 1], weight)
    before = (iota((rows, rows), 1) < iota((rows, rows), 0)).astype(BF)
    slot = dot32(before, named.astype(BF))
    chosen = jnp.where(slot == (place % MOST).astype(F32), named, 0.0)
    for h in range(HALVES):
        mine = jnp.where((place // MOST) % HALVES == h, chosen, 0.0)
        pick_ref[h * rows : (h + 1) * rows, :] = mine.astype(BF)
        high, low = high_low(mine * weight)
        weigh_ref[h * rows : (h + 1) * rows, :] = high
        weigh_ref[(HALVES + h) * rows : (HALVES + h + 1) * rows, :] = low

    def onto(x, w_ref):
        return lax.dot_general(
            x, w_ref[...], (((1,), (1,)), ((), ())), preferred_element_type=F32
        )

    normed = rms_scale(tokens_ref[...], first_gain_ref[...]).astype(BF)
    decay_low = jnp.tanh(onto(normed, decay_down_ref)).astype(BF)
    decay_pre = decay_base_ref[...] + dot32(decay_low, decay_up_ref[...])
    below = jnp.maximum(-decay_pre, 0.0) + jnp.log1p(jnp.exp(-jnp.abs(decay_pre)))
    rate_low = onto(normed, rate_down_ref).astype(BF)
    learn_pre = rate_base_ref[...] + dot32(rate_low, rate_up_ref[...])

    width = scale_ref.shape[1]
    heads = width // HEAD
    both = rows * heads
    own = (iota((rows, heads, LANES), 2) // HEAD) == (iota((rows, heads, LANES), 1) % CORES)
    head = iota((rows, heads, LANES), 1)

    def by_head(x):
        laid = jnp.zeros((rows, heads, LANES), F32)
        for i in range(width // LANES):
            piece = x[:, i * LANES : (i + 1) * LANES][:, None, :]
            laid = jnp.where(own & (head // CORES == i), piece, laid)
        laid = laid.reshape(both, LANES)
        return laid + pltpu.roll(laid, HEAD, 1)

    decay_out[...] = by_head(jnp.exp(-jnp.exp(-below - 0.5)))
    learn_out[...] = by_head(jax.nn.sigmoid(learn_pre))
    scale_out[...] = by_head(jnp.broadcast_to(scale_ref[...], (rows, width)))
    gain_out[...] = by_head(jnp.broadcast_to(gain_ref[...], (rows, width)))


def prepare(total, heads, own_routes, own_weights, tokens, *others):
    rows = tokens.shape[0]
    laid = pltpu.HBM((rows * heads, LANES), F32)
    return pl.pallas_call(
        prepare_kernel,
        in_specs=whole(3 + len(others)),
        out_specs=whole(6),
        out_shape=[
            pltpu.HBM((HALVES * rows, total), BF),
            pltpu.HBM((2 * HALVES * rows, total), BF),
        ]
        + [laid] * 4,
        compiler_params=room(8),
        cost_estimate=pl.CostEstimate(flops=10**9, transcendentals=0, bytes_accessed=10**6),
        name="prepare",
    )(own_routes, own_weights, in_hbm(tokens), *(in_hbm(x) for x in others))


def slices_kernel(spot_ref, tokens_ref, gain_ref, out_ref, normed_ref):
    normed_ref[...] = rms_scale(tokens_ref[...], gain_ref[...]).astype(BF)
    depth = out_ref.shape[2]
    plane = spot_ref[0] // (RING * GROUP)
    for step in range(PLANES):
        at = pl.multiple_of((plane + step) % PLANES * depth, LANES)
        out_ref[step] = normed_ref[:, pl.ds(at, depth)]


def row_slices(spot, tokens, gain):
    rows, width = tokens.shape
    return pl.pallas_call(
        slices_kernel,
        in_specs=[pl.BlockSpec(memory_space=pltpu.SMEM)] + whole(2),
        out_specs=whole(1)[0],
        out_shape=jax.ShapeDtypeStruct((PLANES, rows, width // PLANES), BF),
        scratch_shapes=[pltpu.VMEM((rows, width), BF)],
        compiler_params=room(8),
        name="slices",
    )(spot, in_hbm(tokens), in_hbm(gain[None, :]))


def columns_kernel(receptance_ref, key_ref, value_ref, out_ref, parts_ref, piece_ref, sems):
    sources = (receptance_ref, key_ref, value_ref)
    reads = [
        pltpu.make_async_copy(s, parts_ref.at[i], sems.at[i]) for i, s in enumerate(sources)
    ]
    for read in reads:
        read.start()
    for read in reads:
        read.wait()
    for m in range(GROUP):
        at = slice(m * LANES, (m + 1) * LANES)
        piece_ref[m] = jnp.concatenate([parts_ref[i, :, at] for i in range(3)], axis=1)
    writes = [
        pltpu.make_async_copy(piece_ref, out_ref.at[pl.ds(a * GROUP, GROUP)], sems.at[3 + a])
        for a in range(out_ref.shape[0] // GROUP)
    ]
    for write in writes:
        write.start()
    for write in writes:
        write.wait()


def weight_columns(receptance, key, value, plane):
    rows = key.shape[0]
    hbm = pl.BlockSpec(memory_space=pltpu.HBM)
    return pl.pallas_call(
        columns_kernel,
        in_specs=[hbm] * 3,
        out_specs=hbm,
        out_shape=pltpu.HBM((plane, rows, 3 * LANES), BF),
        scratch_shapes=[
            pltpu.VMEM((3,) + key.shape, BF),
            pltpu.VMEM((GROUP, rows, 3 * LANES), BF),
            pltpu.SemaphoreType.DMA((3 + plane // GROUP,)),
        ],
        compiler_params=room(8),
        name="columns",
    )(in_hbm(receptance), in_hbm(key), in_hbm(value))


def project_kernel(spot_ref, same_ref, other_ref, weight_ref, out_ref):
    rows = out_ref.shape[1]
    spot = spot_ref[0]
    plane = spot // (GROUP * RING)
    place = spot // CORES % RING
    for side, ref in enumerate((same_ref, other_ref)):
        sums = dot32(ref[...], weight_ref[...]).astype(BF)
        core = (spot + side) % CORES
        for step in range(RING):
            for back in range(PLANES):
                member = (plane + PLANES - back) % PLANES * GROUP
                member = member + (place + RING - step) % RING * CORES + core
                at = (step * PLANES + back) * rows
                out_ref[member] = sums[at : at + rows]


def project(spot, same, other, weights, rows):
    return pl.pallas_call(
        project_kernel,
        in_specs=[pl.BlockSpec(memory_space=pltpu.SMEM)] + whole(3),
        out_specs=whole(1)[0],
        out_shape=pltpu.HBM((PLANES * GROUP, rows, weights.shape[1]), BF),
        compiler_params=room(16),
        name="project",
    )(spot, in_hbm(same), in_hbm(other), in_hbm(weights))


def read_kernel(
    sent_ref,
    decay_ref,
    learn_ref,
    scale_ref,
    gain_ref,
    state_ref,
    output_ref,
    tokens_ref,
    second_gain_ref,
    pick_ref,
    residual_ref,
    second_ref,
    chunks_ref,
    known_ref,
    value_ref,
    key_ref,
    taken_ref,
    held_ref,
    laid_ref,
    made_ref,
    sems,
    write_sems,
):
    rows, heads, lanes = state_ref.shape
    reads = []
    for c in range(lanes // COLUMN):
        at = pl.ds(c * COLUMN, COLUMN)
        reads.append(
            pltpu.make_async_copy(state_ref.at[:, :, at], held_ref.at[:, :, at], sems.at[c])
        )
    fetch = pltpu.make_async_copy(output_ref, laid_ref, sems.at[lanes // COLUMN])
    for read in reads:
        read.start()
    fetch.start()
    both = rows * heads
    members = sent_ref.shape[0] // PLANES
    chunk = COLUMN
    row = iota((both, members), 0)
    member = iota((both, members), 1)
    mine = ((row // heads) == (member % rows)) & ((row % heads) // CORES == member // rows)
    sent = sum(sent_ref[z * members : (z + 1) * members, :].astype(F32) for z in range(PLANES))
    owned = dot32(mine.astype(BF), sent.astype(BF))
    side = (iota((both, LANES), 0) % CORES) == (iota((both, LANES), 1) // HEAD)
    first_half = iota((both, LANES), 1) < HEAD

    def part(i):
        return jnp.where(side, owned[:, i * LANES : (i + 1) * LANES], 0.0)

    def twice(x):
        return x + pltpu.roll(x, HEAD, 1)

    def over_keys(x):
        return jnp.sum(x, axis=-1, keepdims=True) * 0.5

    reader2 = twice(part(0))
    key2 = twice(part(1))
    value = part(2)
    scaled = key2 * scale_ref[...]
    dir2 = scaled / jnp.sqrt(over_keys(scaled * scaled) + 1.0)
    taken2 = dir2 * learn_ref[...]
    kept2 = decay_ref[...] * reader2
    removed2 = jnp.zeros((both, LANES), F32)
    readout2 = jnp.zeros((both, LANES), F32)
    for c in range(lanes // chunk):
        removing, reading = [], []
        reads[c].wait()
        for j in range(chunk // LANES):
            at = c * chunk + j * LANES
            state = held_ref[:, :, at : at + LANES].reshape(both, LANES)
            removing.append((state * dir2).astype(BF))
            reading.append((state * kept2).astype(BF))
        fold = fold_matrix(c)
        removed2 = removed2 + dot32(jnp.concatenate(removing, axis=1), fold)
        readout2 = readout2 + dot32(jnp.concatenate(reading, axis=1), fold)
    readout2 = (
        readout2 - removed2 * over_keys(taken2 * reader2) + twice(value) * over_keys(key2 * reader2)
    )
    high, low = high_low(removed2)
    known_ref[...] = jnp.where(first_half, high.astype(F32), low.astype(F32)).astype(BF)
    value_ref[...] = value.astype(BF)
    key_ref[...] = key2
    taken_ref[...] = taken2

    centre = jnp.mean(readout2, axis=-1, keepdims=True)
    apart = readout2 - centre
    spread_of = jnp.mean(apart * apart, axis=-1, keepdims=True)
    mixed2 = apart * lax.rsqrt(spread_of + GROUP_EPS) * gain_ref[...]
    width = heads * HEAD
    own_head = (iota((both, width), 0) % heads) == (iota((both, width), 1) // HEAD)
    laid = jnp.where(own_head, jnp.concatenate([mixed2] * (width // LANES), axis=1), 0.0)
    collect = (iota((rows, both), 0) == iota((rows, both), 1) // heads).astype(BF)
    mixed = dot32(collect, laid.astype(BF)).astype(BF)
    fetch.wait()
    residual = (tokens_ref[...].astype(F32) + dot32(mixed, laid_ref[...])).astype(BF)
    second = rms_scale(residual, second_gain_ref[...]).astype(BF)
    residual_ref[...] = residual
    second_ref[...] = second
    half = second.shape[1] // HALVES
    halves = jnp.concatenate([second[:, h * half : (h + 1) * half] for h in range(HALVES)], axis=0)
    writes = []
    for b in range(made_ref.shape[0] // BLOCK):
        at = pl.ds(b * BLOCK, BLOCK)
        made_ref[at, :] = lax.dot_general(
            pick_ref[:, at], halves, (((0,), (0,)), ((), ())), preferred_element_type=F32
        ).astype(BF)
        write = pltpu.make_async_copy(made_ref.at[at], chunks_ref.at[at], write_sems.at[b])
        write.start()
        writes.append(write)
    for write in writes:
        write.wait()


def read_heads(sent, decay, learn, scale, gain, state, w_output, tokens, second_gain, pick):
    rows, heads, lanes = state.shape
    width = tokens.shape[1]
    both = rows * heads
    hbm = pl.BlockSpec(memory_space=pltpu.HBM)
    return pl.pallas_call(
        read_kernel,
        in_specs=whole(5) + [hbm, hbm] + whole(3),
        out_specs=whole(2) + [hbm] + whole(4),
        out_shape=[
            jax.ShapeDtypeStruct((rows, width), BF),
            jax.ShapeDtypeStruct((rows, width), BF),
            pltpu.HBM((pick.shape[1], width // HALVES), BF),
            jax.ShapeDtypeStruct((both, LANES), BF),
            jax.ShapeDtypeStruct((both, LANES), BF),
            jax.ShapeDtypeStruct((both, LANES), F32),
            jax.ShapeDtypeStruct((both, LANES), F32),
        ],
        compiler_params=room(32),
        scratch_shapes=[
            pltpu.VMEM(state.shape, F32),
            pltpu.VMEM(w_output.shape, BF),
            pltpu.VMEM((pick.shape[1], width // HALVES), BF),
            pltpu.SemaphoreType.DMA((lanes // COLUMN + 1,)),
            pltpu.SemaphoreType.DMA((pick.shape[1] // BLOCK,)),
        ],
        name="read",
    )(
        in_hbm(sent),
        in_hbm(decay),
        in_hbm(learn),
        in_hbm(scale),
        in_hbm(gain),
        in_hbm(state),
        in_hbm(w_output),
        in_hbm(tokens),
        in_hbm(second_gain[None, :]),
        in_hbm(pick),
    )


def write_kernel(known_ref, value_ref, key_ref, taken_ref, decay_ref, state_ref, out_ref):
    rows, heads, lanes = state_ref.shape
    both = rows * heads
    chunk = COLUMN
    for c in range(lanes // chunk):
        spread = spread_matrix(c)
        removed_wide = dot32(known_ref[...], spread)
        value_wide = dot32(value_ref[...], spread)
        for j in range(chunk // LANES):
            at = c * chunk + j * LANES
            sub = slice(j * LANES, (j + 1) * LANES)
            state = (
                state_ref[:, :, at : at + LANES].reshape(both, LANES) * decay_ref[...]
                - removed_wide[:, sub] * taken_ref[...]
                + value_wide[:, sub] * key_ref[...]
            )
            out_ref[:, :, at : at + LANES] = state.reshape(rows, heads, LANES)


def write_heads(known, value, key, taken, decay, state):
    return pl.pallas_call(
        write_kernel,
        in_specs=whole(6),
        out_specs=whole(1)[0],
        out_shape=jax.ShapeDtypeStruct(state.shape, F32),
        cost_estimate=pl.CostEstimate(flops=8 * 10**9, transcendentals=0, bytes_accessed=10**7),
        compiler_params=room(24),
        name="write",
    )(known, value, key, taken, decay, state)


def expert_kernel(chunks_ref, gate_ref, up_ref, down_ref, out_ref, made_ref, sems):
    half = chunks_ref.shape[1]
    kept = BLOCK // HALVES
    row = iota((BLOCK, BLOCK), 0)
    column = iota((BLOCK, BLOCK), 1)
    slot = row % kept
    split = (column == slot // MOST * (MOST * HALVES) + row // kept * MOST + slot % MOST).astype(BF)
    back = iota((BLOCK, BLOCK), 1)
    back_slot = back % kept
    source = back_slot // MOST * (MOST * HALVES) + back // kept * MOST + back_slot % MOST
    join = (iota((BLOCK, BLOCK), 0) == source).astype(BF)
    inputs = []
    for b in range(chunks_ref.shape[0] // BLOCK):
        apart = dot32(split, chunks_ref[b * BLOCK : (b + 1) * BLOCK, :]).astype(BF)
        inputs.append(jnp.concatenate([apart[:kept], apart[kept:]], axis=1))
    inputs = jnp.concatenate(inputs, axis=0)
    hidden = gated_units(inputs, gate_ref[...], up_ref[...])
    writes = []
    for b in range(chunks_ref.shape[0] // BLOCK):
        mine = dot32(hidden[b * kept : (b + 1) * kept], down_ref[...]).astype(BF)
        stacked = jnp.concatenate([mine[:, :half], mine[:, half:]], axis=0)
        at = pl.ds(b * BLOCK, BLOCK)
        made_ref[at, :] = dot32(join, stacked).astype(BF)
        write = pltpu.make_async_copy(made_ref.at[at], out_ref.at[at], sems.at[b])
        write.start()
        writes.append(write)
    for write in writes:
        write.wait()


def run_expert(chunks, gate, up, down):
    return pl.pallas_call(
        expert_kernel,
        in_specs=whole(4),
        out_specs=pl.BlockSpec(memory_space=pltpu.HBM),
        out_shape=pltpu.HBM(chunks.shape, BF),
        scratch_shapes=[
            pltpu.VMEM(chunks.shape, BF),
            pltpu.SemaphoreType.DMA((chunks.shape[0] // BLOCK,)),
        ],
        compiler_params=room(24),
        name="expert",
    )(chunks, gate, up, down)


def combine_kernel(weigh_ref, returned_ref, residual_ref, shared_ref, out_ref, held_ref, sems):
    rows = residual_ref.shape[0]
    total, half = returned_ref.shape
    blocks = [pl.ds(i * BLOCK, BLOCK) for i in range(total // BLOCK)]
    reads = [
        pltpu.make_async_copy(returned_ref.at[at], held_ref.at[at], sems.at[i])
        for i, at in enumerate(blocks)
    ]
    for read in reads:
        read.start()
    parts = jnp.zeros((weigh_ref.shape[0], half), F32)
    for at, read in zip(blocks, reads):
        read.wait()
        parts = parts + dot32(weigh_ref[:, at], held_ref[at, :])
    parts = parts[: HALVES * rows] + parts[HALVES * rows :]
    for h in range(HALVES):
        at = slice(h * half, (h + 1) * half)
        out_ref[:, at] = (
            residual_ref[:, at].astype(F32)
            + shared_ref[:, at]
            + parts[h * rows : (h + 1) * rows]
        ).astype(BF)


def combine(weigh, returned, residual, shared):
    return pl.pallas_call(
        combine_kernel,
        in_specs=whole(1) + [pl.BlockSpec(memory_space=pltpu.HBM)] + whole(2),
        out_specs=whole(1)[0],
        out_shape=jax.ShapeDtypeStruct(residual.shape, BF),
        scratch_shapes=[
            pltpu.VMEM(returned.shape, BF),
            pltpu.SemaphoreType.DMA((returned.shape[0] // BLOCK,)),
        ],
        compiler_params=room(8),
        name="combine",
    )(weigh, returned, residual, shared)


def exchanged(x, groups=None):
    return lax.all_to_all(
        x, "ep", split_axis=0, concat_axis=0, tiled=True, axis_index_groups=groups
    )


def group_slices(slices, devices):
    def hop(stride, step):
        ends = []
        for d in range(devices):
            place = d // stride % RING
            ends.append((d, d + ((place + step) % RING - place) * stride))
        return ends

    rows = [slices[0]]
    for step in range(1, PLANES):
        rows.append(lax.ppermute(slices[step], "ep", hop(GROUP * RING, step)))
    column = jnp.concatenate(rows, axis=0)
    rows = [column]
    for step in range(1, RING):
        rows.append(lax.ppermute(column, "ep", hop(CORES, step)))
    same = jnp.concatenate(rows, axis=0)
    return same, lax.ppermute(same, "ep", [(d, d ^ 1) for d in range(devices)])


def per_device(
    tokens,
    recurrent_state,
    first_gain,
    w_receptance,
    w_key,
    w_value,
    decay_down,
    decay_up,
    decay_base,
    rate_down,
    rate_up,
    rate_base,
    key_scale,
    head_gain,
    w_output,
    second_gain,
    shared_gate,
    shared_up,
    shared_down,
    expert_gate,
    expert_up,
    expert_down,
    routes,
    route_weights,
):
    rows, width = tokens.shape
    heads = recurrent_state.shape[1]
    half = width // HALVES
    devices = lax.axis_size("ep")
    me = lax.axis_index("ep")

    plane = RING * GROUP
    slices = row_slices(me[None], tokens, first_gain)
    columns = weight_columns(w_receptance, w_key, w_value, plane)
    same_z = [list(range(first, first + plane)) for first in range(0, devices, plane)]
    same_y = [
        [z * plane + y * GROUP + m for z in range(PLANES) for m in range(GROUP)]
        for y in range(RING)
    ]
    weights = exchanged(columns, same_z)
    same, other = group_slices(slices, devices)

    own_routes = lax.dynamic_slice_in_dim(routes, me * rows, rows, 0)
    own_weights = lax.dynamic_slice_in_dim(route_weights, me * rows, rows, 0)
    pick, weigh, decay, learn, scale, gain = prepare(
        devices * MOST * HALVES,
        heads,
        own_routes,
        own_weights,
        tokens,
        first_gain[None, :],
        decay_down.T,
        decay_up,
        decay_base[None, :],
        rate_down.T,
        rate_up,
        rate_base[None, :],
        key_scale[None, :],
        head_gain[None, :],
    )
    sums = project(me[None], same, other, weights.reshape(plane * rows, 3 * LANES), rows)
    sent = exchanged(sums, same_y)
    residual, second, outgoing, known, value, key, taken = read_heads(
        sent.reshape(plane * rows, 3 * LANES),
        decay,
        learn,
        scale,
        gain,
        recurrent_state,
        w_output,
        tokens,
        second_gain,
        pick,
    )
    received = exchanged(outgoing.reshape(devices, MOST * HALVES, half))
    shared = dot32(gated_units(second, shared_gate, shared_up), shared_down)
    new_state = write_heads(known, value, key, taken, decay, recurrent_state)
    produced = run_expert(
        received.reshape(devices * MOST * HALVES, half), expert_gate[0], expert_up[0], expert_down[0]
    )
    returned = exchanged(produced.reshape(devices, MOST * HALVES, half))
    new_tokens = combine(
        weigh, returned.reshape(devices * MOST * HALVES, half), residual, shared
    )
    return (new_tokens, new_state)


def solution(mesh):
    row = P("ep", None)
    block = P("ep", None, None)
    copied = P()
    in_specs = (
        (row, block, copied, row, row, row)
        + (copied,) * 13
        + (block, block, block, copied, copied)
    )
    return jax.shard_map(
        per_device, mesh=mesh, in_specs=in_specs, out_specs=(row, block), check_vma=False
    )
```

time: 154 us -> 137 us (0.89)
  other arithmetic: 9.03 us -> 0.01 us
  waiting for transfers between devices: 41.3 us -> 33.5 us
  Pallas kernels: 22.7 us -> 27 us
  matrix products: 8.35 us -> 4.34 us
  local copies, waits for them, and re-layouts: 7.37 us -> 5.52 us
    convert_element_type x6 -> x0, other arithmetic: 4.89 us -> none  [the longest x1 2.7 us: mix_heads(): fold = (lane[:, None] // HEAD == entry[None, :]).astype(BF)]
    ppermute x4 -> x7, starting transfers between devices: 5.25 us -> 10 us  [the longest x3 5.34 us: group_slices(): rows.append(lax.ppermute(slices[step], 'ep', hop(GROUP * RING, step)))]
    pallas_call x3 -> x8, Pallas kernels: 22.7 us -> 27 us  [the longest x1 7.48 us: read_heads(): pl.pallas_call(read_kernel, in_specs=whole(5) + [hbm, hbm] + whole(3), ou...]
    dot_general x6 -> x2, matrix products: 8.35 us -> 4.34 us  [dot32(): return jnp.dot(a, b, preferred_element_type=F32)]
    ppermute x4 -> x7, waiting for transfers between devices: 11.8 us -> 7.86 us  [the longest x3 6.69 us: group_slices(): rows.append(lax.ppermute(column, 'ep', hop(CORES, step)))]
    all_to_all x3, waiting for transfers between devices: 29.5 us -> 25.7 us  [exchanged(): lax.all_to_all(x, 'ep', split_axis=0, concat_axis=0, tiled=True, axis_ind...]
    all_to_all x3, starting transfers between devices: 22.4 us -> 19 us  [exchanged(): lax.all_to_all(x, 'ep', split_axis=0, concat_axis=0, tiled=True, axis_ind...]
    concatenate x3 -> x1, other arithmetic: 2.36 us -> 0.01 us  [group_slices(): column = jnp.concatenate(rows, axis=0)]
  transfers between devices with their start and end apart: 7 -> 10, of which waited for: 4 -> 4; matrix products, arithmetic and copies ran while one was open for 13% -> 4% of each run, Pallas kernels for 0% -> 6%
where the time goes in v3:
time: 137 us; the launch traced here: 136 us
  blocking collectives  36 us (26%)
  waiting for transfers between devices  33.5 us (24%)
  starting transfers between devices  29 us (21%)
  Pallas kernels  27 us (20%)
  local copies, waits for them, and re-layouts  5.52 us (4%)
  matrix products  4.34 us (3%)
    all_to_all x1, blocking collectives, exchanged(): lax.all_to_all(x, 'ep', split_axis=0, concat_axis=0, tiled=True, axis_ind...  36 us
    all_to_all x3, waiting for transfers between devices, exchanged(): lax.all_to_all(x, 'ep', split_axis=0, concat_axis=0, tiled=True, axis_ind...  25.7 us
    all_to_all x3, starting transfers between devices, exchanged(): lax.all_to_all(x, 'ep', split_axis=0, concat_axis=0, tiled=True, axis_ind...  19 us
    pallas_call x1, Pallas kernels, read_heads(): pl.pallas_call(read_kernel, in_specs=whole(5) + [hbm, hbm] + whole(3), ou...  7.48 us
    ppermute x3, waiting for transfers between devices, group_slices(): rows.append(lax.ppermute(column, 'ep', hop(CORES, step)))  6.69 us
    pallas_call x1, Pallas kernels, run_expert(): pl.pallas_call(expert_kernel, in_specs=whole(4), out_specs=pl.BlockSpec(m...  5.62 us
    ppermute x3, starting transfers between devices, group_slices(): rows.append(lax.ppermute(slices[step], 'ep', hop(GROUP * RING, step)))  5.34 us
    dot_general x2, matrix products, dot32(): return jnp.dot(a, b, preferred_element_type=F32)  4.34 us
  transfers between devices with their start and end apart: 10, of which 4 were waited for; matrix products, arithmetic and copies ran while one was open for 4% of the time, Pallas kernels for 6%

profile of v3, /device:TPU:1, one launch (start us, length us, event | category | flops | bytes accessed | tf_op | source)
XLA Modules:
  0.0 136.5 jit_solution(16731577710916403046)
XLA Ops:
  0.6 0.0 copy-start
  0.6 1.1 slices.1
  1.8 4.6 %collective-permute-start.2 = (bf16[16,512]{1,0:T(8,128)(2,1)S(1)}, bf16[16,512]{1,0:T(8,128)(2,1)S(1)}, u32[]{:S(2)}, u32[]{:S(2)}) collective-permute-start(bf16[16,512]{1,0:T(8,128)(2,1)S(1)} %get-tuple-element.29), channel_id=1, source_target_pairs={{0,96},{1,97},{2,98},{3,99},{4,100},{5,101},{6,102},{7,103},{8,104... | collective-permute-start | bytes 49160 | tf_op jit(solution)/shard_map/ppermute | solution.py:533
  6.4 0.0 collective-permute-start.1
  6.4 0.7 collective-permute-start
  7.1 1.6 %columns.1 = bf16[32,16,384]{2,1,0:T(8,128)(2,1)} custom-call(bf16[16,1024]{1,0:T(8,128)(2,1)} %receptance_ref.1, bf16[16,1024]{1,0:T(8,128)(2,1)} %key_ref.1, bf16[16,1024]{1,0:T(8,128)(2,1)} %value_ref.1), custom_call_target="tpu_custom_call" | custom-call | tf_op jit(solution)/shard_map/columns/pallas_call | solution.py:206
  8.7 8.6 %all-to-all-start = ((bf16[32,16,384]{2,1,0:T(8,128)(2,1)}), bf16[32,16,384]{2,1,0:T(8,128)(2,1)S(1)}, u32[]{:S(2)}, u32[]{:S(2)}) async-start(bf16[32,16,384]{2,1,0:T(8,128)(2,1)} %columns.1), calls=%async_computation | async-start | bytes 786432 | tf_op jit(solution)/shard_map/all_to_all | solution.py:518
  17.4 0.0 collective-permute-done.2
  17.4 0.0 collective-permute-done.1
  17.4 0.0 collective-permute-done
  17.4 2.6 %collective-permute-start.5 = (bf16[64,512]{1,0:T(8,128)(2,1)S(1)}, bf16[64,512]{1,0:T(8,128)(2,1)S(1)}, u32[]{:S(2)}, u32[]{:S(2)}) collective-permute-start(bf16[64,512]{1,0:T(8,128)(2,1)S(1)} %pad_maximum_fusion), channel_id=1, source_target_pairs={{0,6},{1,7},{2,0},{3,1},{4,2},{5,3},{6,4},{7,5},{8,14},{9,15},{10,... | collective-permute-start | bytes 196616 | tf_op jit(solution)/shard_map/ppermute | solution.py:537
  20.0 0.6 collective-permute-start.4
  20.6 0.6 collective-permute-start.3
  21.2 6.7 %collective-permute-done.3 = bf16[64,512]{1,0:T(8,128)(2,1)S(1)} collective-permute-done((bf16[64,512]{1,0:T(8,128)(2,1)S(1)}, bf16[64,512]{1,0:T(8,128)(2,1)S(1)}, u32[]{:S(2)}, u32[]{:S(2)}) %collective-permute-start.3) | collective-permute-done | bytes 65568 | tf_op jit(solution)/shard_map/ppermute | solution.py:537
  27.9 0.0 collective-permute-done.4
  27.9 0.0 collective-permute-done.5
  27.9 0.0 copy-start.9
  28.0 0.9 collective-permute-start.6
  28.8 1.2 collective-permute-done.6.other_ref
  30.0 0.0 copy-start.10
  30.0 0.0 all-to-all-done
  30.0 0.0 copy-start.7
  30.0 0.0 copy-done.9
  30.0 0.7 copy-done.10
  30.7 0.1 copy-done.7
  30.8 2.3 %project.1 = bf16[32,16,384]{2,1,0:T(8,128)(2,1)} custom-call(s32[1]{0:T(128)} %bitcast.7.spot_ref, bf16[256,512]{1,0:T(8,128)(2,1)} %copy-done.9, bf16[256,512]{1,0:T(8,128)(2,1)} %copy-done.10, bf16[512,384]{1,0:T(8,128)(2,1)} %bitcast.39), custom_call_target="tpu_custom_call" | custom-call | tf_op jit(solution)/shard_map/project/pallas_call | solution.py:238
  33.1 4.9 %all-to-all-start.1 = ((bf16[32,16,384]{2,1,0:T(8,128)(2,1)}), bf16[32,16,384]{2,1,0:T(8,128)(2,1)S(1)}, u32[]{:S(2)}, u32[]{:S(2)}) async-start(bf16[32,16,384]{2,1,0:T(8,128)(2,1)} %project.1), calls=%async_computation.1 | async-start | bytes 786432 | tf_op jit(solution)/shard_map/all_to_all | solution.py:518
  38.1 0.8 constant_dynamic-slice_fusion
  38.9 0.1 copy.29.weights_ref
  38.9 0.8 constant_dynamic-slice_fusion.1
  39.7 0.1 copy.28.routes_ref
  39.8 2.9 %prepare.1 = (bf16[32,1024]{1,0:T(8,128)(2,1)}, bf16[64,1024]{1,0:T(8,128)(2,1)}, f32[256,128]{1,0:T(8,128)}, f32[256,128]{1,0:T(8,128)}, f32[256,128]{1,0:T(8,128)}, /*index=5*/f32[256,128]{1,0:T(8,128)}) custom-call(s32[16,4]{1,0:T(8,128)S(1)} %copy.28.routes_ref, f32[16,4]{1,0:T(8,128)S(1)} %copy.29.weights_ref, bf16[16,2048]{1,0:T(8,128)(2,1)} %tokens_ref.5, ...), custom_call_target="tpu_custom_call" | custom-call | flops 1000000000 | bytes 1000000 | tf_op jit(solution)/shard_map/prepare/pallas_call | solution.py:144
  42.7 5.6 %all-to-all-done.1 = bf16[32,16,384]{2,1,0:T(8,128)(2,1)S(1)} async-done(((bf16[32,16,384]{2,1,0:T(8,128)(2,1)}), bf16[32,16,384]{2,1,0:T(8,128)(2,1)S(1)}, u32[]{:S(2)}, u32[]{:S(2)}) %all-to-all-start.1) | async-done | bytes 393248 | tf_op jit(solution)/shard_map/all_to_all | solution.py:518
  48.2 0.0 copy-start.8
  48.2 0.7 copy-done.8
  49.0 0.0 copy-start.4
  49.0 7.5 %read.1 = (bf16[16,2048]{1,0:T(8,128)(2,1)S(1)}, bf16[16,2048]{1,0:T(8,128)(2,1)S(1)}, bf16[1024,1024]{1,0:T(8,128)(2,1)}, bf16[256,128]{1,0:T(8,128)(2,1)S(1)},...) custom-call(bf16[512,384]{1,0:T(8,128)(2,1)} %bitcast.40, ...), custom_call_target="tpu_custom_call" | custom-call | tf_op jit(solution)/shard_map/read/pallas_call | solution.py:366
  56.5 0.0 copy-start.2
  56.5 0.0 copy-start.3
  56.5 36.0 %all_to_all.20 = bf16[128,8,1024]{2,1,0:T(8,128)(2,1)S(1)} all-to-all(bf16[128,8,1024]{2,1,0:T(8,128)(2,1)} %bitcast.38), channel_id=1, replica_groups=mesh['ep'=128] {'ep'}, dimensions={0} | all-to-all | bytes 4194304 | tf_op jit(solution)/shard_map/all_to_all | solution.py:518
  92.5 0.0 copy-done.4
  92.5 0.0 copy-done.2
  92.5 0.0 copy-done.3
  92.5 5.6 %expert.1 = bf16[1024,1024]{1,0:T(8,128)(2,1)} custom-call(bf16[1024,1024]{1,0:T(8,128)(2,1)S(1)} %bitcast.33, bf16[2048,512]{1,0:T(8,128)(2,1)S(1)} %bitcast.34, bf16[2048,512]{1,0:T(8,128)(2,1)S(1)} %bitcast.35, bf16[512,2048]{1,0:T(8,128)(2,1)S(1)} %bitcast.36), custom_call_target="tpu_custom_call" | custom-call | tf_op jit(solution)/shard_map/expert/pallas_call | solution.py:464
  98.2 5.5 %all-to-all-start.3 = ((bf16[128,8,1024]{2,1,0:T(8,128)(2,1)}), bf16[128,8,1024]{2,1,0:T(8,128)(2,1)}, u32[]{:S(2)}, u32[]{:S(2)}) async-start(bf16[128,8,1024]{2,1,0:T(8,128)(2,1)} %bitcast.37), calls=%async_computation.3 | async-start | bytes 4194304 | tf_op jit(solution)/shard_map/all_to_all | solution.py:518
  103.7 2.0 %fusion.9 = f32[16,512]{1,0:T(8,128)S(1)} fusion(bf16[16,2048]{1,0:T(8,128)(2,1)S(1)} %get-tuple-element.23, bf16[2048,512]{1,0:T(8,128)(2,1)} %param.40), kind=kOutput, calls=%fused_computation.24 | convolution fusion | flops 33554432 | bytes 2195456 | tf_op jit(solution)/shard_map/dot_general | solution.py:32
  105.6 0.0 copy-done
  105.6 0.0 copy-start.5
  105.6 2.4 %fusion.1.shared_ref = f32[16,2048]{1,0:T(8,128)S(1)} fusion(bf16[512,2048]{1,0:T(8,128)(2,1)S(1)} %copy-done, bf16[16,2048]{1,0:T(8,128)(2,1)S(1)} %get-tuple-element.23, bf16[2048,512]{1,0:T(8,128)(2,1)} %param.41, f32[16,512]{1,0:T(8,128)S(1)} %fusion.9), kind=kOutput, calls=%fused_computation.2 | convolution fusion | flops 67158016 | bytes 4423680 | tf_op jit(solution)/shard_map/dot_general | solution.py:32
  108.0 0.0 copy-done.5
  108.0 0.0 copy-start.1
  108.0 2.2 %copy-done.1 = f32[16,16,4096]{2,1,0:T(8,128)S(1)} copy-done((f32[16,16,4096]{2,1,0:T(8,128)S(1)}, f32[16,16,4096]{2,1,0:T(8,128)}, u32[]{:S(2)}) %copy-start.1) | copy-done | bytes 4194328
  110.2 0.0 copy-start.6
  110.2 3.6 %write.1 = f32[16,16,4096]{2,1,0:T(8,128)} custom-call(bf16[256,128]{1,0:T(8,128)(2,1)S(1)} %get-tuple-element.24.known_ref, bf16[256,128]{1,0:T(8,128)(2,1)S(1)} %get-tuple-element.25.value_ref, f32[256,128]{1,0:T(8,128)S(1)} %get-tuple-element.26.key_ref, f32[256,128]{1,0:T(8,128)S(1)} %get-tuple-element.27.taken_ref, f32[256,128]{1,0:T(8,128)S(1)} %copy-done.5, ...), custom_call_target="tpu_custom_call" | custom-call | flops 8000000000 | bytes 10000000 | tf_op jit(solution)/shard_map/write/pallas_call | solution.py:422
  113.8 20.1 %all-to-all-done.3 = bf16[128,8,1024]{2,1,0:T(8,128)(2,1)} async-done(((bf16[128,8,1024]{2,1,0:T(8,128)(2,1)}), bf16[128,8,1024]{2,1,0:T(8,128)(2,1)}, u32[]{:S(2)}, u32[]{:S(2)}) %all-to-all-start.3) | async-done | bytes 2097184 | tf_op jit(solution)/shard_map/all_to_all | solution.py:518
  133.9 0.0 copy-done.6
  133.9 2.4 %combine.1 = bf16[16,2048]{1,0:T(8,128)(2,1)} custom-call(bf16[64,1024]{1,0:T(8,128)(2,1)S(1)} %copy-done.6, bf16[1024,1024]{1,0:T(8,128)(2,1)} %bitcast.21.returned_ref, bf16[16,2048]{1,0:T(8,128)(2,1)S(1)} %get-tuple-element.22.residual_ref, f32[16,2048]{1,0:T(8,128)S(1)} %fusion.1.shared_ref), custom_call_target="tpu_custom_call" | custom-call | tf_op jit(solution)/shard_map/combine/pallas_call | solution.py:503
  (9 shorter events, 0.0 us)
Async XLA Ops:
  0.6 105.0 %copy-start = (bf16[512,2048]{1,0:T(8,128)(2,1)S(1)}, bf16[512,2048]{1,0:T(8,128)(2,1)}, u32[]{:S(2)}) copy-start(bf16[512,2048]{1,0:T(8,128)(2,1)} %param.42) | copy-start | bytes 6291460
  1.8 15.6 %collective-permute-start.2 = (bf16[16,512]{1,0:T(8,128)(2,1)S(1)}, bf16[16,512]{1,0:T(8,128)(2,1)S(1)}, u32[]{:S(2)}, u32[]{:S(2)}) collective-permute-start(bf16[16,512]{1,0:T(8,128)(2,1)S(1)} %get-tuple-element.29), channel_id=1, source_target_pairs={{0,96},{1,97},{2,98},{3,99},{4,100},{5,101},{6,102},{7,103},{8,104... | collective-permute-start | bytes 49160 | tf_op jit(solution)/shard_map/ppermute | solution.py:533
  6.4 11.0 %collective-permute-start.1 = (bf16[16,512]{1,0:T(8,128)(2,1)S(1)}, bf16[16,512]{1,0:T(8,128)(2,1)S(1)}, u32[]{:S(2)}, u32[]{:S(2)}) collective-permute-start(bf16[16,512]{1,0:T(8,128)(2,1)S(1)} %get-tuple-element.30), channel_id=1, source_target_pairs={{0,64},{1,65},{2,66},{3,67},{4,68},{5,69},{6,70},{7,71},{8,72},{9,... | collective-permute-start | bytes 49160 | tf_op jit(solution)/shard_map/ppermute | solution.py:533
  6.4 11.0 %collective-permute-start = (bf16[16,512]{1,0:T(8,128)(2,1)S(1)}, bf16[16,512]{1,0:T(8,128)(2,1)S(1)}, u32[]{:S(2)}, u32[]{:S(2)}) collective-permute-start(bf16[16,512]{1,0:T(8,128)(2,1)S(1)} %get-tuple-element.31), channel_id=1, source_target_pairs={{0,32},{1,33},{2,34},{3,35},{4,36},{5,37},{6,38},{7,39},{8,40},{9,... | collective-permute-start | bytes 49160 | tf_op jit(solution)/shard_map/ppermute | solution.py:533
  8.7 21.3 %all-to-all-start = ((bf16[32,16,384]{2,1,0:T(8,128)(2,1)}), bf16[32,16,384]{2,1,0:T(8,128)(2,1)S(1)}, u32[]{:S(2)}, u32[]{:S(2)}) async-start(bf16[32,16,384]{2,1,0:T(8,128)(2,1)} %columns.1), calls=%async_computation | async-start | bytes 786432 | tf_op jit(solution)/shard_map/all_to_all | solution.py:518
  17.4 10.5 %collective-permute-start.5 = (bf16[64,512]{1,0:T(8,128)(2,1)S(1)}, bf16[64,512]{1,0:T(8,128)(2,1)S(1)}, u32[]{:S(2)}, u32[]{:S(2)}) collective-permute-start(bf16[64,512]{1,0:T(8,128)(2,1)S(1)} %pad_maximum_fusion), channel_id=1, source_target_pairs={{0,6},{1,7},{2,0},{3,1},{4,2},{5,3},{6,4},{7,5},{8,14},{9,15},{10,... | collective-permute-start | bytes 196616 | tf_op jit(solution)/shard_map/ppermute | solution.py:537
  20.0 7.9 %collective-permute-start.4 = (bf16[64,512]{1,0:T(8,128)(2,1)S(1)}, bf16[64,512]{1,0:T(8,128)(2,1)S(1)}, u32[]{:S(2)}, u32[]{:S(2)}) collective-permute-start(bf16[64,512]{1,0:T(8,128)(2,1)S(1)} %pad_maximum_fusion), channel_id=1, source_target_pairs={{0,4},{1,5},{2,6},{3,7},{4,0},{5,1},{6,2},{7,3},{8,12},{9,13},{10,... | collective-permute-start | bytes 196616 | tf_op jit(solution)/shard_map/ppermute | solution.py:537
  20.6 7.3 %collective-permute-start.3 = (bf16[64,512]{1,0:T(8,128)(2,1)S(1)}, bf16[64,512]{1,0:T(8,128)(2,1)S(1)}, u32[]{:S(2)}, u32[]{:S(2)}) collective-permute-start(bf16[64,512]{1,0:T(8,128)(2,1)S(1)} %pad_maximum_fusion), channel_id=1, source_target_pairs={{0,2},{1,3},{2,4},{3,5},{4,6},{5,7},{6,0},{7,1},{8,10},{9,11},{10,... | collective-permute-start | bytes 196616 | tf_op jit(solution)/shard_map/ppermute | solution.py:537
  27.9 2.0 %copy-start.9 = (bf16[256,512]{1,0:T(8,128)(2,1)}, bf16[256,512]{1,0:T(8,128)(2,1)S(1)}, u32[]{:S(2)}) copy-start(bf16[256,512]{1,0:T(8,128)(2,1)S(1)} %constant_dynamic-update-slice_fusion.same_ref) | copy-start | bytes 786436
  28.0 2.0 %collective-permute-start.6 = (bf16[256,512]{1,0:T(8,128)(2,1)S(1)}, bf16[256,512]{1,0:T(8,128)(2,1)S(1)}, u32[]{:S(2)}, u32[]{:S(2)}) collective-permute-start(bf16[256,512]{1,0:T(8,128)(2,1)S(1)} %constant_dynamic-update-slice_fusion.same_ref), channel_id=1, source_target_pairs={{0,1},{1,0},{2,3},{3,2},{4,5},{5,4},{6,7},{7,6},{8,9},{9,8},{10,11... | collective-permute-start | bytes 786440 | tf_op jit(solution)/shard_map/ppermute | solution.py:539
  30.0 0.7 copy-start.10
  30.0 0.8 copy-start.7
  33.1 15.1 %all-to-all-start.1 = ((bf16[32,16,384]{2,1,0:T(8,128)(2,1)}), bf16[32,16,384]{2,1,0:T(8,128)(2,1)S(1)}, u32[]{:S(2)}, u32[]{:S(2)}) async-start(bf16[32,16,384]{2,1,0:T(8,128)(2,1)} %project.1), calls=%async_computation.1 | async-start | bytes 786432 | tf_op jit(solution)/shard_map/all_to_all | solution.py:518
  48.2 0.7 copy-start.8
  49.0 43.5 %copy-start.4 = (bf16[1,512,2048]{2,1,0:T(8,128)(2,1)S(1)}, bf16[1,512,2048]{2,1,0:T(8,128)(2,1)}, u32[]{:S(2)}) copy-start(bf16[1,512,2048]{2,1,0:T(8,128)(2,1)} %param.45) | copy-start | bytes 6291460
  56.5 36.1 %copy-start.2 = (bf16[1,2048,512]{2,1,0:T(8,128)(2,1)S(1)}, bf16[1,2048,512]{2,1,0:T(8,128)(2,1)}, u32[]{:S(2)}) copy-start(bf16[1,2048,512]{2,1,0:T(8,128)(2,1)} %param.43) | copy-start | bytes 6291460
  56.5 36.1 %copy-start.3 = (bf16[1,2048,512]{2,1,0:T(8,128)(2,1)S(1)}, bf16[1,2048,512]{2,1,0:T(8,128)(2,1)}, u32[]{:S(2)}) copy-start(bf16[1,2048,512]{2,1,0:T(8,128)(2,1)} %param.44) | copy-start | bytes 6291460
  98.2 35.7 %all-to-all-start.3 = ((bf16[128,8,1024]{2,1,0:T(8,128)(2,1)}), bf16[128,8,1024]{2,1,0:T(8,128)(2,1)}, u32[]{:S(2)}, u32[]{:S(2)}) async-start(bf16[128,8,1024]{2,1,0:T(8,128)(2,1)} %bitcast.37), calls=%async_computation.3 | async-start | bytes 4194304 | tf_op jit(solution)/shard_map/all_to_all | solution.py:518
  105.6 2.4 %copy-start.5 = (f32[256,128]{1,0:T(8,128)S(1)}, f32[256,128]{1,0:T(8,128)}, u32[]{:S(2)}) copy-start(f32[256,128]{1,0:T(8,128)} %get-tuple-element.16.decay_ref) | copy-start | bytes 393220
  108.0 2.2 %copy-start.1 = (f32[16,16,4096]{2,1,0:T(8,128)S(1)}, f32[16,16,4096]{2,1,0:T(8,128)}, u32[]{:S(2)}) copy-start(f32[16,16,4096]{2,1,0:T(8,128)} %state_ref.3) | copy-start | bytes 12582916
  110.2 23.7 %copy-start.6 = (bf16[64,1024]{1,0:T(8,128)(2,1)S(1)}, bf16[64,1024]{1,0:T(8,128)(2,1)}, u32[]{:S(2)}) copy-start(bf16[64,1024]{1,0:T(8,128)(2,1)} %get-tuple-element.15.weigh_ref) | copy-start | bytes 393220
